TPU v7x, 32 devices: a whole 2x2x4 slice. The times are simulated.
32 devices in a mesh: sp: 8 (over z, x), tp: 4 (over y, core).
Axes of the slice: x: 2, y: 2, z: 4, core: 2. Of those that a mesh axis runs over, the one named last changes fastest.
Arguments:
- tokens: bfloat16 [4096, 4096], P(('sp', 'tp')), may hold values from -6 to 6
- lock_projector: bfloat16 [4096, 1024], P(None, 'tp'), may hold values from -0.01171875 to 0.01171875
- value_weight: bfloat16 [4096, 2048], P(None, 'tp'), may hold values from -0.0234375 to 0.0234375
- decay_weight: bfloat16 [4096, 1024], P(None, 'tp'), may hold values from -0.09375 to 0.09375
- decay_offset: float32 [1024], P('tp'), may hold values from -3.5 to 0
- fresh_question: bfloat16 [16, 64], P('tp'), may hold values from -6 to 6
Outputs:
- state_cache: bfloat16 [16, 64, 128], P('tp', 'sp')
- first_read: bfloat16 [16, 128], P('tp')
All inputs are finite; a program needn't handle non-finite values.
Results may differ from a plain program's by a relative error of at most 0.0034.
Values may be sent and summed in bfloat16 or wider, within the bound.
No kernel may reach another device: no remote copies, remote signals or barrier semaphores. Data moves between devices by JAX's collectives and lax.ppermute only.
A program may use at most 64 MiB of HBM per device.

v0:
```python
import functools
import math

import jax
import jax.numpy as jnp
from jax import lax
from jax.experimental import pallas as pl
from jax.experimental.pallas import tpu as pltpu
from jax.sharding import PartitionSpec as P


CUE_WIDTH = 64
DV = 128
DECAY_TAU = 16.0
ROW_PARTS = (2, 3, 3)
COL_PARTS = (3, 1)
LATE = len(COL_PARTS)
VMEM_LIMIT = 8 * 1024 * 1024


F32 = jnp.float32
BF16 = jnp.bfloat16
EXACT = lax.Precision.HIGHEST


def swap(count, bit):
    return [(i, i ^ bit) for i in range(count)]


def products(x, weights, start=0):
    stop = start + x.shape[1]
    return [jnp.dot(x, w[start:stop, :], preferred_element_type=F32) for w in weights]


def project(sums, offset, log_length):
    keys, values, pre = sums
    z = pre + offset + log_length
    log_decay = (jnp.minimum(z, 0.0) - jnp.log1p(jnp.exp(-jnp.abs(z)))) / DECAY_TAU
    return keys.astype(BF16), values.astype(BF16), log_decay


def later_within(log_decay, sizes):
    rows = log_decay.shape[0]
    i = lax.broadcasted_iota(jnp.int32, (rows, rows), 0)
    j = lax.broadcasted_iota(jnp.int32, (rows, rows), 1)
    mask = j > i
    edge = 0
    for size in sizes[:-1]:
        edge += size
        mask = mask & ((i >= edge) == (j >= edge))
    return jnp.dot(mask.astype(F32), log_decay, precision=EXACT, preferred_element_type=F32)


def weigh(keys, after):
    exact = keys.astype(F32) * jnp.exp(after)
    high = exact.astype(BF16)
    return high, (exact - high.astype(F32)).astype(BF16)


def outer(values, weighted):
    high, low = weighted
    heads = high.shape[1] // CUE_WIDTH
    group = min(2, heads)
    cols = group * CUE_WIDTH
    parts = []
    for g in range(heads // group):
        w = jnp.concatenate([p[:, g * cols : (g + 1) * cols] for p in (high, low)], axis=1)
        v = values[:, g * group * DV : (g + 1) * group * DV]
        full = lax.dot_general(v, w, (((0,), (0,)), ((), ())), preferred_element_type=F32)
        full = full[:, :cols] + full[:, cols:]
        kept = full[:DV]
        if group == 2:
            lane = lax.broadcasted_iota(jnp.int32, kept.shape, 1)
            kept = jnp.where(lane < CUE_WIDTH, kept, full[DV:])
        parts.append(kept)
    return parts[0] if len(parts) == 1 else jnp.concatenate(parts, axis=1)


def payload_sds(heads, heard):
    rows = 3 + 3 * heads if heard else 3
    width = max(heads * CUE_WIDTH, DV)
    return jax.ShapeDtypeStruct((DV + rows + -rows % 8, width), BF16)


def split(exact):
    parts, rest = [], exact
    for _ in range(3):
        parts.append(rest.astype(BF16).astype(F32))
        rest = rest - parts[-1]
    return parts


def widen(x, width):
    extra = width - x.shape[1]
    return jnp.concatenate([x, jnp.zeros((x.shape[0], extra), x.dtype)], axis=1) if extra else x


def pack(out, state, total, heard=None):
    width = out.shape[1]
    rows = [widen(p, width) for p in split(total)]
    if heard is not None:
        for part in split(heard):
            part = widen(part, width)
            rows += [part[h : h + 1] for h in range(part.shape[0])]
    row = lax.broadcasted_iota(jnp.int32, (out.shape[0] - DV, width), 0)
    tail = jnp.zeros(row.shape, F32)
    for n, value in enumerate(rows):
        tail = jnp.where(row == n, value, tail)
    out[:DV, :] = widen(state.astype(BF16), width)
    out[DV:, :] = tail.astype(BF16)


def unpack(ref, key_cols):
    tail = ref[DV:, :].astype(F32)
    total = tail[0:1] + tail[1:2] + tail[2:3]
    return ref[:DV, :key_cols].astype(F32), total[:, :key_cols], tail


def heard_of(tail, heads):
    parts = [tail[3 + n * heads : 3 + (n + 1) * heads, :DV] for n in range(3)]
    return parts[0] + parts[1] + parts[2]


def ask_kernel(question, out):
    row = lax.broadcasted_iota(jnp.int32, out.shape, 0)
    lane = lax.broadcasted_iota(jnp.int32, out.shape, 1)
    heads = question.shape[0]
    asked = jnp.concatenate([question[...].astype(F32)] * heads, axis=1) * CUE_WIDTH ** (-0.5)
    if out.shape[0] > heads:
        spare = jnp.zeros((out.shape[0] - heads, out.shape[1]), F32)
        asked = jnp.concatenate([asked, spare], axis=0)
    out[...] = jnp.where(lax.div(lane, CUE_WIDTH) == row, asked, 0.0)


def against(left, state):
    return lax.dot_general(
        left, state, (((1,), (1,)), ((), ())), precision=EXACT, preferred_element_type=F32
    )


def cut_kernel(tokens, *refs, cuts):
    sems = refs[-1]
    copies = [
        pltpu.make_async_copy(tokens.at[lo:hi, left:right], out, sems.at[n])
        for n, ((lo, hi, left, right), out) in enumerate(zip(cuts, refs))
    ]
    for copy in copies:
        copy.start()
    for copy in copies:
        copy.wait()


def near_kernel(x0, x1, wk, wv, wd, off, s_out, l_out, *, log_length):
    core = lax.rem(lax.axis_index("tp"), 2)
    rows = x0.shape[0]
    x = jnp.concatenate([x0[...], x1[...]], axis=0)
    keys, values, log_decay = project(products(x, (wk, wv, wd)), off[...], log_length)
    after = later_within(log_decay, [rows, rows])
    own = after[0:1] + log_decay[0:1]
    sib = after[rows : rows + 1] + log_decay[rows : rows + 1]
    own_tail = jnp.where(core == 0, sib, 0.0)
    sib_tail = jnp.where(core == 0, 0.0, own)
    row = lax.broadcasted_iota(jnp.int32, after.shape, 0)
    after = after + jnp.where(row < rows, own_tail, sib_tail)
    s_out[...] = outer(values, weigh(keys, after))
    l_out[...] = own + sib


def early_kernel(*refs, log_length, pieces, split):
    sides = []
    for side in (refs[:pieces], refs[pieces : 2 * pieces]):
        whole = [ref[...] for ref in side]
        if split:
            whole = whole[:-LATE] + [jnp.concatenate(whole[-LATE:], axis=1)]
        sides.append(jnp.concatenate(whole, axis=0))
    wk, wv, wd, off, s_a, s_b, l_a, l_b = refs[2 * pieces :]
    rows = sides[0].shape[0]
    x = jnp.concatenate(sides, axis=0)
    keys, values, log_decay = project(products(x, (wk, wv, wd)), off[...], log_length)
    after = later_within(log_decay, [rows, rows])
    weighted = weigh(keys, after)
    s_a[...] = outer(values[:rows], [w[:rows] for w in weighted])
    s_b[...] = outer(values[rows:], [w[rows:] for w in weighted])
    l_a[...] = after[0:1] + log_decay[0:1]
    l_b[...] = after[rows : rows + 1] + log_decay[rows : rows + 1]


def partial_kernel(xa, xb, wk, wv, wd, *outs):
    x = jnp.concatenate([xa[...], xb[...]], axis=0)
    for out, value in zip(outs, products(x, (wk, wv, wd))):
        out[...] = value


def late_kernel(xa, xb, ks, vs, ds, wk, wv, wd, off, *refs, log_length, blocks, here, parts):
    states = refs[: len(blocks)]
    totals = refs[len(blocks) : 2 * len(blocks)]
    out = refs[2 * len(blocks)]
    place = lax.axis_index("tp")
    core = lax.rem(place, 2)
    chip = lax.div(place, 2)
    rows = xa.shape[0]

    def position(block):
        if block is None:
            return chip * (2 * parts)
        bit, part, same = block
        parity = core if same else 1 - core
        return lax.bitwise_xor(chip, bit) * (2 * parts) + parity * parts + part

    x = jnp.concatenate([xa[...], xb[...]], axis=0)
    more = products(x, (wk, wv, wd), wk.shape[0] - x.shape[1])
    sums = [s[...] + m for s, m in zip((ks, vs, ds), more)]
    keys, values, log_decay = project(sums, off[...], log_length)
    after = later_within(log_decay, [rows, rows])
    own = [
        after[0:1] + log_decay[0:1],
        after[rows : rows + 1] + log_decay[rows : rows + 1],
    ]
    every = [(position(b), totals[n][...]) for n, b in enumerate(blocks)]
    mine = [position(here + (True,)), position(here + (False,))]
    every += list(zip(mine, own))

    def later_of(pos):
        acc = jnp.zeros_like(own[0])
        for p, t in every:
            acc = acc + jnp.where(p > pos, t, 0.0)
        return acc

    row = lax.broadcasted_iota(jnp.int32, after.shape, 0)
    after = after + jnp.where(row < rows, later_of(mine[0]), later_of(mine[1]))
    state = outer(values, weigh(keys, after))
    total = own[0] + own[1]
    for n in range(len(blocks)):
        pos, t = every[n]
        state = state + states[n][...] * jnp.exp(later_of(pos))
        total = total + t
    pack(out, state, total)


def merge_kernel(asked, *refs, bits):
    count = 2 ** len(bits)
    out, exact = refs[count:]
    key_cols = asked.shape[1]
    parts = [unpack(ref, key_cols)[:2] for ref in refs[:count]]
    for n, bit in enumerate(bits):
        turned = lax.bitwise_and(lax.axis_index("sp"), bit) != 0
        parts = [
            tuple(jnp.where(turned, x, y) for x, y in zip(parts[k ^ (1 << n)], parts[k]))
            for k in range(count)
        ]
    state, total = parts[0]
    for s, t in parts[1:]:
        state = state * jnp.exp(t) + s
        total = total + t
    exact[...] = state
    heads = key_cols // CUE_WIDTH
    last = out.shape[0] > DV + 8
    pack(out, state, total, against(asked[...], state)[:heads] if last else None)


def final_kernel(asked, mine, other, exact, cache, read, *, bit):
    heads, kept, _ = cache.shape
    key_cols = asked.shape[1]
    earlier = lax.bitwise_and(lax.axis_index("sp"), bit) == 0
    s_m, l_m, tail_m = unpack(mine, key_cols)
    s_o, l_o, tail_o = unpack(other, key_cols)
    fading = jnp.exp(jnp.where(earlier, l_o, l_m))
    first = jnp.where(earlier, s_m, s_o) * fading
    state = jnp.where(earlier, exact[...] * fading + s_o, first + exact[...])
    rows = heads * kept
    rows += -rows % 8
    row = lax.broadcasted_iota(jnp.int32, (rows, key_cols), 0)
    lane = lax.broadcasted_iota(jnp.int32, (rows, key_cols), 1)
    start = lax.axis_index("sp") * kept
    column = lax.div(row, kept) * CUE_WIDTH + start + lax.rem(row, kept)
    chosen = ((row < heads * kept) & (lane == column)).astype(F32)
    result = against(chosen, state)
    for h in range(heads):
        cache[h] = result[h * kept : (h + 1) * kept].astype(BF16)
    heard = against(asked[...], first)[:heads]
    heard = heard + heard_of(jnp.where(earlier, tail_o, tail_m), heads)
    mean = jnp.mean(heard * heard, axis=-1, keepdims=True)
    read[...] = (heard * lax.rsqrt(mean + 1.0)).astype(BF16)


VM = pl.BlockSpec(memory_space=pltpu.VMEM)


def call(kernel, out_shape, in_specs, scratch=(), flops=0):
    return pl.pallas_call(
        kernel,
        out_shape=out_shape,
        in_specs=in_specs,
        out_specs=jax.tree.map(lambda _: VM, out_shape),
        scratch_shapes=list(scratch),
        cost_estimate=pl.CostEstimate(flops=flops, bytes_accessed=0, transcendentals=0),
        compiler_params=pltpu.CompilerParams(vmem_limit_bytes=VMEM_LIMIT),
    )


def whole(sp, tp, tokens, wk, wv, wd, decay_offset, fresh_question):
    rows, width = tokens.shape
    key_cols, value_cols = wk.shape[1], wv.shape[1]
    heads = key_cols // CUE_WIDTH
    cols = 2 * key_cols + value_cols
    log_length = math.log(rows * tp * sp)
    offset = decay_offset.reshape(1, key_cols)
    sds = jax.ShapeDtypeStruct
    state_sds = sds((DV, key_cols), F32)
    total_sds = sds((1, key_cols), F32)

    edges = [rows * sum(ROW_PARTS[:n]) // sum(ROW_PARTS) for n in range(len(ROW_PARTS) + 1)]
    sides = [width * sum(COL_PARTS[:n]) // sum(COL_PARTS) for n in range(LATE + 1)]
    cuts = [(lo, hi, 0, width) for lo, hi in zip(edges[:-2], edges[1:-1])]
    cuts += [(edges[-2], edges[-1], lo, hi) for lo, hi in zip(sides[:-1], sides[1:])]
    held = pltpu.with_memory_space_constraint(tokens, pltpu.HBM)
    pieces = []
    for some in (cuts[:1], cuts[1:]):
        pieces += call(
            functools.partial(cut_kernel, cuts=tuple(some)),
            tuple(pltpu.VMEM((h - l, r - c), BF16) for l, h, c, r in some),
            [pl.BlockSpec(memory_space=pltpu.HBM)],
            [pltpu.SemaphoreType.DMA((len(some),))],
        )(held)
    far = {}
    for bit in range(1, tp // 2):
        for part, piece in enumerate(pieces):
            far[bit, part] = lax.ppermute(piece, "tp", swap(tp, 2 * bit))
    sibling = lax.ppermute(tokens, "tp", swap(tp, 1))

    s_near, l_near = call(
        functools.partial(near_kernel, log_length=log_length),
        (state_sds, total_sds),
        [VM] * 6,
        flops=4 * rows * width * cols,
    )(tokens, sibling, wk, wv, wd, offset)

    asked = call(ask_kernel, sds((heads + -heads % 8, key_cols), F32), [VM])(fresh_question)

    blocks, states, totals = [None], [s_near], [l_near]
    pairs = {}
    for bit, part in far:
        pairs[bit, part] = (far[bit, part], lax.ppermute(far[bit, part], "tp", swap(tp, 1)))
    final_bit = tp // 2 - 1
    last = [pairs[final_bit, len(cuts) - LATE + n] for n in range(LATE)]
    for bit in range(1, tp // 2):
        taken = [pairs[bit, n] for n in range(len(cuts) - (LATE if bit == final_bit else 0))]
        inputs = [pair[side] for side in (0, 1) for pair in taken]
        far_rows = edges[-2] if bit == final_bit else rows
        s_a, s_b, l_a, l_b = call(
            functools.partial(
                early_kernel,
                log_length=log_length,
                pieces=len(taken),
                split=bit != final_bit,
            ),
            (state_sds, state_sds, total_sds, total_sds),
            [VM] * (len(inputs) + 4),
            flops=4 * far_rows * width * cols,
        )(*inputs, wk, wv, wd, offset)
        blocks += [(bit, 0, True), (bit, 0, False)]
        states += [s_a, s_b]
        totals += [l_a, l_b]
    late_rows = 2 * (edges[-1] - edges[-2])
    sums = call(
        partial_kernel,
        tuple(sds((late_rows, w.shape[1]), F32) for w in (wk, wv, wd)),
        [VM] * 5,
        flops=2 * late_rows * sides[1] * cols,
    )(*last[0], wk, wv, wd)
    payload = call(
        functools.partial(
            late_kernel, log_length=log_length, blocks=tuple(blocks), here=(final_bit, 1), parts=2
        ),
        payload_sds(heads, sp == 2),
        [VM] * (9 + 2 * len(blocks)),
        flops=2 * late_rows * (width - sides[1]) * cols,
    )(*last[1], *sums, wk, wv, wd, offset, *states, *totals)

    bits = [1 << n for n in range(sp.bit_length() - 1)]
    while len(bits) > 1:
        take = 2 if len(bits) > 2 else 1
        group, bits = bits[:take], bits[take:]
        others = []
        for k in range(1, 2**take):
            far_bits = sum(b for n, b in enumerate(group) if k >> n & 1)
            others.append(lax.ppermute(payload, "sp", swap(sp, far_bits)))
        payload, exact = call(
            functools.partial(merge_kernel, bits=tuple(group)),
            (payload_sds(heads, len(bits) == 1), state_sds),
            [VM] * (2 + len(others)),
        )(asked, payload, *others)
    other = lax.ppermute(payload, "sp", swap(sp, bits[0]))
    return call(
        functools.partial(final_kernel, bit=bits[0]),
        (sds((heads, CUE_WIDTH // sp, DV), BF16), sds((heads, DV), BF16)),
        [VM] * 4,
    )(asked, payload, other, exact)


def solution(mesh):
    sp, tp = mesh.shape["sp"], mesh.shape["tp"]
    in_specs = (
        P(("sp", "tp"), None),
        P(None, "tp"),
        P(None, "tp"),
        P(None, "tp"),
        P("tp"),
        P("tp", None),
    )
    out_specs = (P("tp", "sp", None), P("tp", None))
    return jax.shard_map(
        functools.partial(whole, sp, tp),
        mesh=mesh,
        in_specs=in_specs,
        out_specs=out_specs,
        check_vma=False,
    )
```

profile of v0, /device:TPU:0, one launch (start us, length us, event | category | flops | bytes accessed | tf_op | source)
XLA Modules:
  0.0 61.4 jit_solution(13482982663798222385)
XLA Ops:
  0.6 0.6 collective-permute-start.4
  1.2 1.2 %shard_map.78 = (bf16[48,4096]{1,0:T(8,128)(2,1)S(1)}, bf16[48,3072]{1,0:T(8,128)(2,1)S(1)}, bf16[48,1024]{1,0:T(8,128)(2,1)S(1)}) custom-call(bf16[128,4096]{1,0:T(8,128)(2,1)} %tokens.3), custom_call_target="tpu_custom_call" | custom-call | tf_op jit(solution)/shard_map/pallas_call | solution.py:319
  2.4 2.7 %collective-permute-start.6 = (bf16[48,4096]{1,0:T(8,128)(2,1)S(1)}, bf16[48,4096]{1,0:T(8,128)(2,1)S(1)}, u32[]{:S(2)}, u32[]{:S(2)}) collective-permute-start(bf16[48,4096]{1,0:T(8,128)(2,1)S(1)} %get-tuple-element.22), channel_id=1, source_target_pairs={{0,2},{1,3},{2,0},{3,1},{4,6},{5,7},{6,4},{7,5},{8,10},{9,11},{10,... | collective-permute-start | bytes 1179656 | tf_op jit(solution)/shard_map/ppermute | solution.py:328
  5.0 0.1 collective-permute-start.2
  5.1 1.0 %shard_map.81 = bf16[32,4096]{1,0:T(8,128)(2,1)S(1)} custom-call(bf16[128,4096]{1,0:T(8,128)(2,1)} %tokens.3), custom_call_target="tpu_custom_call" | custom-call | tf_op jit(solution)/shard_map/pallas_call | solution.py:319
  6.1 2.0 %collective-permute-start.5 = (bf16[32,4096]{1,0:T(8,128)(2,1)S(1)}, bf16[32,4096]{1,0:T(8,128)(2,1)S(1)}, u32[]{:S(2)}, u32[]{:S(2)}) collective-permute-start(bf16[32,4096]{1,0:T(8,128)(2,1)S(1)} %shard_map.81), channel_id=1, source_target_pairs={{0,2},{1,3},{2,0},{3,1},{4,6},{5,7},{6,4},{7,5},{8,10},{9,11},{10,... | collective-permute-start | bytes 786440 | tf_op jit(solution)/shard_map/ppermute | solution.py:328
  8.1 6.9 %collective-permute-done.6.refs_1_ = bf16[48,4096]{1,0:T(8,128)(2,1)S(1)} collective-permute-done((bf16[48,4096]{1,0:T(8,128)(2,1)S(1)}, bf16[48,4096]{1,0:T(8,128)(2,1)S(1)}, u32[]{:S(2)}, u32[]{:S(2)}) %collective-permute-start.6) | collective-permute-done | bytes 393248 | tf_op jit(solution)/shard_map/ppermute | solution.py:328
  15.0 0.0 collective-permute-start.8
  15.0 6.3 %collective-permute-done.2.xa = bf16[48,3072]{1,0:T(8,128)(2,1)S(1)} collective-permute-done((bf16[48,3072]{1,0:T(8,128)(2,1)S(1)}, bf16[48,3072]{1,0:T(8,128)(2,1)S(1)}, u32[]{:S(2)}, u32[]{:S(2)}) %collective-permute-start.2) | collective-permute-done | bytes 294944 | tf_op jit(solution)/shard_map/ppermute | solution.py:328
  21.3 5.3 %collective-permute-done.5.refs_0_ = bf16[32,4096]{1,0:T(8,128)(2,1)S(1)} collective-permute-done((bf16[32,4096]{1,0:T(8,128)(2,1)S(1)}, bf16[32,4096]{1,0:T(8,128)(2,1)S(1)}, u32[]{:S(2)}, u32[]{:S(2)}) %collective-permute-start.5) | collective-permute-done | bytes 262176 | tf_op jit(solution)/shard_map/ppermute | solution.py:328
  26.6 1.7 %collective-permute-start = (bf16[48,1024]{1,0:T(8,128)(2,1)S(1)}, bf16[48,1024]{1,0:T(8,128)(2,1)S(1)}, u32[]{:S(2)}, u32[]{:S(2)}) collective-permute-start(bf16[48,1024]{1,0:T(8,128)(2,1)S(1)} %get-tuple-element.16), channel_id=1, source_target_pairs={{0,2},{1,3},{2,0},{3,1},{4,6},{5,7},{6,4},{7,5},{8,10},{9,11},{10,... | collective-permute-start | bytes 294920 | tf_op jit(solution)/shard_map/ppermute | solution.py:328
  28.4 3.5 %collective-permute-done.xa = bf16[48,1024]{1,0:T(8,128)(2,1)S(1)} collective-permute-done((bf16[48,1024]{1,0:T(8,128)(2,1)S(1)}, bf16[48,1024]{1,0:T(8,128)(2,1)S(1)}, u32[]{:S(2)}, u32[]{:S(2)}) %collective-permute-start) | collective-permute-done | bytes 98336 | tf_op jit(solution)/shard_map/ppermute | solution.py:328
  31.9 0.0 copy-start
  31.9 2.2 %copy-done = bf16[4096,512]{1,0:T(8,128)(2,1)S(1)} copy-done((bf16[4096,512]{1,0:T(8,128)(2,1)S(1)}, bf16[4096,512]{1,0:T(8,128)(2,1)}, u32[]{:S(2)}) %copy-start) | copy-done | bytes 4194328
  34.0 1.6 %copy-done.3 = bf16[4096,256]{1,0:T(8,128)(2,1)S(1)} copy-done((bf16[4096,256]{1,0:T(8,128)(2,1)S(1)}, bf16[4096,256]{1,0:T(8,128)(2,1)}, u32[]{:S(2)}) %copy-start.3) | copy-done | bytes 2097176
  35.6 1.1 %shard_map.79 = (f32[96,256]{1,0:T(8,128)S(1)}, f32[96,512]{1,0:T(8,128)S(1)}, f32[96,256]{1,0:T(8,128)S(1)}) custom-call(bf16[48,3072]{1,0:T(8,128)(2,1)S(1)} %collective-permute-done.2.xa, bf16[48,3072]{1,0:T(8,128)(2,1)S(1)} %collective-permute-done.3.xb, bf16[4096,256]{1,0:T(8,128)(2,1)S(1)} %copy-done.2, bf16[4096,512]{1,0:T(8,128)(2,1)S(1)} %copy-done, ...), custom_call_target="tpu_custom_call" | custom-call | flops 603979776 | tf_op jit(solution)/shard_map/pallas_call | solution.py:365
  36.8 1.0 %copy-done.1 = bf16[4096,512]{1,0:T(8,128)(2,1)S(1)} copy-done((bf16[4096,512]{1,0:T(8,128)(2,1)S(1)}, bf16[4096,512]{1,0:T(8,128)(2,1)}, u32[]{:S(2)}) %copy-start.1) | copy-done | bytes 4194328
  37.8 2.4 %shard_map.82 = (f32[128,256]{1,0:T(8,128)S(1)}, f32[128,256]{1,0:T(8,128)S(1)}, f32[1,256]{1,0:T(1,128)S(1)}, f32[1,256]{1,0:T(1,128)S(1)}) custom-call(bf16[32,4096]{1,0:T(8,128)(2,1)S(1)} %collective-permute-done.5.refs_0_, bf16[48,4096]{1,0:T(8,128)(2,1)S(1)} %collective-permute-done.6.refs_1_, bf16[32,4096]{1,0:T(8,128)(2,1)S(1)} %collective-permute-done.7.refs_2_, ...), custom_call_target="tpu_custom_call" | custom-call | flops 1342177280 | tf_op jit(solution)/shard_map/pallas_call | solution.py:350
  40.2 3.4 %shard_map.80 = (f32[128,256]{1,0:T(8,128)S(1)}, f32[1,256]{1,0:T(1,128)S(1)}) custom-call(bf16[128,4096]{1,0:T(8,128)(2,1)S(1)} %copy-done.5, bf16[128,4096]{1,0:T(8,128)(2,1)S(1)} %collective-permute-done.4.x1, bf16[4096,256]{1,0:T(8,128)(2,1)S(1)} %copy-done.2, bf16[4096,512]{1,0:T(8,128)(2,1)S(1)} %copy-done.1, bf16[4096,256]{1,0:T(8,128)(2,1)S(1)} %copy-done.4, ...), custom_call_target="tpu_custom_call" | custom-call | flops 2147483648 | tf_op jit(solution)/shard_map/pallas_call | solution.py:331
  43.7 0.0 copy-start.7
  43.7 1.1 %shard_map.83.refs_0_ = bf16[136,256]{1,0:T(8,128)(2,1)S(1)} custom-call(bf16[48,1024]{1,0:T(8,128)(2,1)S(1)} %collective-permute-done.xa, bf16[48,1024]{1,0:T(8,128)(2,1)S(1)} %collective-permute-done.1.xb, f32[96,256]{1,0:T(8,128)S(1)} %get-tuple-element.18.ks, f32[96,512]{1,0:T(8,128)S(1)} %get-tuple-element.19.vs, f32[96,256]{1,0:T(8,128)S(1)} %get-tuple-element.20.ds, ...), custom_call_target="tpu_custom_call" | custom-call | flops 201326592 | tf_op jit(solution)/shard_map/pallas_call | solution.py:371
  44.8 1.9 %collective-permute-start.10 = (bf16[136,256]{1,0:T(8,128)(2,1)S(1)}, bf16[136,256]{1,0:T(8,128)(2,1)S(1)}, u32[]{:S(2)}, u32[]{:S(2)}) collective-permute-start(bf16[136,256]{1,0:T(8,128)(2,1)S(1)} %shard_map.83.refs_0_), channel_id=1, source_target_pairs={{0,8},{4,12},{8,0},{12,4},{16,24},{20,28},{24,16},{28,20},{1,9},{5... | collective-permute-start | bytes 208904 | tf_op jit(solution)/shard_map/ppermute | solution.py:387
  46.6 1.4 %collective-permute-start.11 = (bf16[136,256]{1,0:T(8,128)(2,1)S(1)}, bf16[136,256]{1,0:T(8,128)(2,1)S(1)}, u32[]{:S(2)}, u32[]{:S(2)}) collective-permute-start(bf16[136,256]{1,0:T(8,128)(2,1)S(1)} %shard_map.83.refs_0_), channel_id=1, source_target_pairs={{0,12},{4,8},{8,4},{12,0},{16,28},{20,24},{24,20},{28,16},{1,13},{... | collective-permute-start | bytes 208904 | tf_op jit(solution)/shard_map/ppermute | solution.py:387
  48.0 0.3 collective-permute-start.9
  48.3 0.1 shard_map.77.asked
  48.4 1.1 %collective-permute-done.10.refs_2_ = bf16[136,256]{1,0:T(8,128)(2,1)S(1)} collective-permute-done((bf16[136,256]{1,0:T(8,128)(2,1)S(1)}, bf16[136,256]{1,0:T(8,128)(2,1)S(1)}, u32[]{:S(2)}, u32[]{:S(2)}) %collective-permute-start.10) | collective-permute-done | bytes 69664 | tf_op jit(solution)/shard_map/ppermute | solution.py:387
  49.5 2.7 %collective-permute-done.11.refs_3_ = bf16[136,256]{1,0:T(8,128)(2,1)S(1)} collective-permute-done((bf16[136,256]{1,0:T(8,128)(2,1)S(1)}, bf16[136,256]{1,0:T(8,128)(2,1)S(1)}, u32[]{:S(2)}, u32[]{:S(2)}) %collective-permute-start.11) | collective-permute-done | bytes 69664 | tf_op jit(solution)/shard_map/ppermute | solution.py:387
  52.2 1.3 %collective-permute-done.9.refs_1_ = bf16[136,256]{1,0:T(8,128)(2,1)S(1)} collective-permute-done((bf16[136,256]{1,0:T(8,128)(2,1)S(1)}, bf16[136,256]{1,0:T(8,128)(2,1)S(1)}, u32[]{:S(2)}, u32[]{:S(2)}) %collective-permute-start.9) | collective-permute-done | bytes 69664 | tf_op jit(solution)/shard_map/ppermute | solution.py:387
  53.4 0.3 shard_map.84
  53.7 2.7 %collective-permute-start.12 = (bf16[144,256]{1,0:T(8,128)(2,1)S(1)}, bf16[144,256]{1,0:T(8,128)(2,1)S(1)}, u32[]{:S(2)}, u32[]{:S(2)}) collective-permute-start(bf16[144,256]{1,0:T(8,128)(2,1)S(1)} %get-tuple-element.28.mine), channel_id=1, source_target_pairs={{0,16},{4,20},{8,24},{12,28},{16,0},{20,4},{24,8},{28,12},{1,17},{... | collective-permute-start | bytes 221192 | tf_op jit(solution)/shard_map/ppermute | solution.py:393
  56.4 4.0 %collective-permute-done.12.other = bf16[144,256]{1,0:T(8,128)(2,1)S(1)} collective-permute-done((bf16[144,256]{1,0:T(8,128)(2,1)S(1)}, bf16[144,256]{1,0:T(8,128)(2,1)S(1)}, u32[]{:S(2)}, u32[]{:S(2)}) %collective-permute-start.12) | collective-permute-done | bytes 73760 | tf_op jit(solution)/shard_map/ppermute | solution.py:393
  60.4 1.0 %shard_map.85 = (bf16[4,8,128]{2,1,0:T(8,128)(2,1)}, bf16[4,128]{1,0:T(4,128)(2,1)}) custom-call(f32[8,256]{1,0:T(8,128)S(1)} %shard_map.77.asked, bf16[144,256]{1,0:T(8,128)(2,1)S(1)} %get-tuple-element.28.mine, bf16[144,256]{1,0:T(8,128)(2,1)S(1)} %collective-permute-done.12.other, f32[128,256]{1,0:T(8,128)S(1)} %get-tuple-element.29.exact), custom_call_target="tpu_custom_call" | custom-call | tf_op jit(solution)/shard_map/pallas_call | solution.py:394
  (19 shorter events, 0.0 us)
Async XLA Ops:
  0.6 31.2 %copy-start.2 = (bf16[4096,256]{1,0:T(8,128)(2,1)S(1)}, bf16[4096,256]{1,0:T(8,128)(2,1)}, u32[]{:S(2)}) copy-start(bf16[4096,256]{1,0:T(8,128)(2,1)} %wk.5) | copy-start | bytes 6291460
  0.6 39.6 %collective-permute-start.4 = (bf16[128,4096]{1,0:T(8,128)(2,1)}, bf16[128,4096]{1,0:T(8,128)(2,1)S(1)}, u32[]{:S(2)}, u32[]{:S(2)}) collective-permute-start(bf16[128,4096]{1,0:T(8,128)(2,1)} %tokens.3), channel_id=1, source_target_pairs={{0,1},{1,0},{2,3},{3,2},{4,5},{5,4},{6,7},{7,6},{8,9},{9,8},{10,11... | collective-permute-start | bytes 3145736 | tf_op jit(solution)/shard_map/ppermute | solution.py:329
  2.4 12.6 %collective-permute-start.6 = (bf16[48,4096]{1,0:T(8,128)(2,1)S(1)}, bf16[48,4096]{1,0:T(8,128)(2,1)S(1)}, u32[]{:S(2)}, u32[]{:S(2)}) collective-permute-start(bf16[48,4096]{1,0:T(8,128)(2,1)S(1)} %get-tuple-element.22), channel_id=1, source_target_pairs={{0,2},{1,3},{2,0},{3,1},{4,6},{5,7},{6,4},{7,5},{8,10},{9,11},{10,... | collective-permute-start | bytes 1179656 | tf_op jit(solution)/shard_map/ppermute | solution.py:328
  5.0 16.3 %collective-permute-start.2 = (bf16[48,3072]{1,0:T(8,128)(2,1)S(1)}, bf16[48,3072]{1,0:T(8,128)(2,1)S(1)}, u32[]{:S(2)}, u32[]{:S(2)}) collective-permute-start(bf16[48,3072]{1,0:T(8,128)(2,1)S(1)} %get-tuple-element.17), channel_id=1, source_target_pairs={{0,2},{1,3},{2,0},{3,1},{4,6},{5,7},{6,4},{7,5},{8,10},{9,11},{10,... | collective-permute-start | bytes 884744 | tf_op jit(solution)/shard_map/ppermute | solution.py:328
  6.1 20.5 %collective-permute-start.5 = (bf16[32,4096]{1,0:T(8,128)(2,1)S(1)}, bf16[32,4096]{1,0:T(8,128)(2,1)S(1)}, u32[]{:S(2)}, u32[]{:S(2)}) collective-permute-start(bf16[32,4096]{1,0:T(8,128)(2,1)S(1)} %shard_map.81), channel_id=1, source_target_pairs={{0,2},{1,3},{2,0},{3,1},{4,6},{5,7},{6,4},{7,5},{8,10},{9,11},{10,... | collective-permute-start | bytes 786440 | tf_op jit(solution)/shard_map/ppermute | solution.py:328
  15.0 21.8 %collective-permute-start.8 = (bf16[48,4096]{1,0:T(8,128)(2,1)S(1)}, bf16[48,4096]{1,0:T(8,128)(2,1)S(1)}, u32[]{:S(2)}, u32[]{:S(2)}) collective-permute-start(bf16[48,4096]{1,0:T(8,128)(2,1)S(1)} %collective-permute-done.6.refs_1_), channel_id=1, source_target_pairs={{0,1},{1,0},{2,3},{3,2},{4,5},{5,4},{6,7},{7,6},{8,9},{9,8},{10,11... | collective-permute-start | bytes 1179656 | tf_op jit(solution)/shard_map/ppermute | solution.py:343
  21.3 10.5 %collective-permute-start.3 = (bf16[48,3072]{1,0:T(8,128)(2,1)S(1)}, bf16[48,3072]{1,0:T(8,128)(2,1)S(1)}, u32[]{:S(2)}, u32[]{:S(2)}) collective-permute-start(bf16[48,3072]{1,0:T(8,128)(2,1)S(1)} %collective-permute-done.2.xa), channel_id=1, source_target_pairs={{0,1},{1,0},{2,3},{3,2},{4,5},{5,4},{6,7},{7,6},{8,9},{9,8},{10,11... | collective-permute-start | bytes 884744 | tf_op jit(solution)/shard_map/ppermute | solution.py:343
  26.6 10.1 %collective-permute-start.7 = (bf16[32,4096]{1,0:T(8,128)(2,1)S(1)}, bf16[32,4096]{1,0:T(8,128)(2,1)S(1)}, u32[]{:S(2)}, u32[]{:S(2)}) collective-permute-start(bf16[32,4096]{1,0:T(8,128)(2,1)S(1)} %collective-permute-done.5.refs_0_), channel_id=1, source_target_pairs={{0,1},{1,0},{2,3},{3,2},{4,5},{5,4},{6,7},{7,6},{8,9},{9,8},{10,11... | collective-permute-start | bytes 786440 | tf_op jit(solution)/shard_map/ppermute | solution.py:343
  26.6 10.2 %copy-start.6 = (f32[256]{0:T(256)S(1)}, f32[256]{0:T(256)}, u32[]{:S(2)}) copy-start(f32[256]{0:T(256)} %param.10) | copy-start | bytes 3076
  26.6 5.2 %collective-permute-start = (bf16[48,1024]{1,0:T(8,128)(2,1)S(1)}, bf16[48,1024]{1,0:T(8,128)(2,1)S(1)}, u32[]{:S(2)}, u32[]{:S(2)}) collective-permute-start(bf16[48,1024]{1,0:T(8,128)(2,1)S(1)} %get-tuple-element.16), channel_id=1, source_target_pairs={{0,2},{1,3},{2,0},{3,1},{4,6},{5,7},{6,4},{7,5},{8,10},{9,11},{10,... | collective-permute-start | bytes 294920 | tf_op jit(solution)/shard_map/ppermute | solution.py:328
  31.8 11.8 %collective-permute-start.1 = (bf16[48,1024]{1,0:T(8,128)(2,1)S(1)}, bf16[48,1024]{1,0:T(8,128)(2,1)S(1)}, u32[]{:S(2)}, u32[]{:S(2)}) collective-permute-start(bf16[48,1024]{1,0:T(8,128)(2,1)S(1)} %collective-permute-done.xa), channel_id=1, source_target_pairs={{0,1},{1,0},{2,3},{3,2},{4,5},{5,4},{6,7},{7,6},{8,9},{9,8},{10,11... | collective-permute-start | bytes 294920 | tf_op jit(solution)/shard_map/ppermute | solution.py:343
  31.9 2.2 %copy-start = (bf16[4096,512]{1,0:T(8,128)(2,1)S(1)}, bf16[4096,512]{1,0:T(8,128)(2,1)}, u32[]{:S(2)}) copy-start(bf16[4096,512]{1,0:T(8,128)(2,1)} %wv.5) | copy-start | bytes 12582916
  34.0 1.6 %copy-start.3 = (bf16[4096,256]{1,0:T(8,128)(2,1)S(1)}, bf16[4096,256]{1,0:T(8,128)(2,1)}, u32[]{:S(2)}) copy-start(bf16[4096,256]{1,0:T(8,128)(2,1)} %wd.5) | copy-start | bytes 6291460
  35.6 2.2 %copy-start.1 = (bf16[4096,512]{1,0:T(8,128)(2,1)S(1)}, bf16[4096,512]{1,0:T(8,128)(2,1)}, u32[]{:S(2)}) copy-start(bf16[4096,512]{1,0:T(8,128)(2,1)} %wv.5) | copy-start | bytes 12582916
  37.8 2.4 %copy-start.4 = (bf16[4096,256]{1,0:T(8,128)(2,1)S(1)}, bf16[4096,256]{1,0:T(8,128)(2,1)}, u32[]{:S(2)}) copy-start(bf16[4096,256]{1,0:T(8,128)(2,1)} %wd.5) | copy-start | bytes 6291460
  37.8 2.4 %copy-start.5 = (bf16[128,4096]{1,0:T(8,128)(2,1)S(1)}, bf16[128,4096]{1,0:T(8,128)(2,1)}, u32[]{:S(2)}) copy-start(bf16[128,4096]{1,0:T(8,128)(2,1)} %tokens.3) | copy-start | bytes 3145732
  43.7 4.6 %copy-start.7 = (bf16[4,64]{1,0:T(4,128)(2,1)S(1)}, bf16[4,64]{1,0:T(4,128)(2,1)}, u32[]{:S(2)}) copy-start(bf16[4,64]{1,0:T(4,128)(2,1)} %question.1) | copy-start | bytes 1540
  44.8 4.7 %collective-permute-start.10 = (bf16[136,256]{1,0:T(8,128)(2,1)S(1)}, bf16[136,256]{1,0:T(8,128)(2,1)S(1)}, u32[]{:S(2)}, u32[]{:S(2)}) collective-permute-start(bf16[136,256]{1,0:T(8,128)(2,1)S(1)} %shard_map.83.refs_0_), channel_id=1, source_target_pairs={{0,8},{4,12},{8,0},{12,4},{16,24},{20,28},{24,16},{28,20},{1,9},{5... | collective-permute-start | bytes 208904 | tf_op jit(solution)/shard_map/ppermute | solution.py:387
  46.6 5.5 %collective-permute-start.11 = (bf16[136,256]{1,0:T(8,128)(2,1)S(1)}, bf16[136,256]{1,0:T(8,128)(2,1)S(1)}, u32[]{:S(2)}, u32[]{:S(2)}) collective-permute-start(bf16[136,256]{1,0:T(8,128)(2,1)S(1)} %shard_map.83.refs_0_), channel_id=1, source_target_pairs={{0,12},{4,8},{8,4},{12,0},{16,28},{20,24},{24,20},{28,16},{1,13},{... | collective-permute-start | bytes 208904 | tf_op jit(solution)/shard_map/ppermute | solution.py:387
  48.0 5.4 %collective-permute-start.9 = (bf16[136,256]{1,0:T(8,128)(2,1)S(1)}, bf16[136,256]{1,0:T(8,128)(2,1)S(1)}, u32[]{:S(2)}, u32[]{:S(2)}) collective-permute-start(bf16[136,256]{1,0:T(8,128)(2,1)S(1)} %shard_map.83.refs_0_), channel_id=1, source_target_pairs={{0,4},{4,0},{8,12},{12,8},{16,20},{20,16},{24,28},{28,24},{1,5},{5... | collective-permute-start | bytes 208904 | tf_op jit(solution)/shard_map/ppermute | solution.py:387
  53.7 6.6 %collective-permute-start.12 = (bf16[144,256]{1,0:T(8,128)(2,1)S(1)}, bf16[144,256]{1,0:T(8,128)(2,1)S(1)}, u32[]{:S(2)}, u32[]{:S(2)}) collective-permute-start(bf16[144,256]{1,0:T(8,128)(2,1)S(1)} %get-tuple-element.28.mine), channel_id=1, source_target_pairs={{0,16},{4,20},{8,24},{12,28},{16,0},{20,4},{24,8},{28,12},{1,17},{... | collective-permute-start | bytes 221192 | tf_op jit(solution)/shard_map/ppermute | solution.py:393
where the time goes:
time: 61.6 us; the launch traced here: 61.4 us
  waiting for transfers between devices  31 us (50%)
  starting transfers between devices  13.3 us (22%)
  Pallas kernels  11.5 us (19%)
  local copies, waits for them, and re-layouts  4.82 us (8%)
  between operations  0.78 us (1%)
    ppermute x4, waiting for transfers between devices, whole(): far[bit, part] = lax.ppermute(piece, 'tp', swap(tp, 2 * bit))  22 us
    ppermute x4, starting transfers between devices, whole(): far[bit, part] = lax.ppermute(piece, 'tp', swap(tp, 2 * bit))  6.49 us
    ppermute x3, waiting for transfers between devices, whole(): others.append(lax.ppermute(payload, 'sp', swap(sp, far_bits)))  5.03 us
    unnamed x16, local copies, waits for them, and re-layouts  4.82 us
    ppermute x1, waiting for transfers between devices, whole(): other = lax.ppermute(payload, 'sp', swap(sp, bits[0]))  3.95 us
    ppermute x3, starting transfers between devices, whole(): others.append(lax.ppermute(payload, 'sp', swap(sp, far_bits)))  3.55 us
    pallas_call x1, Pallas kernels, whole(): call(functools.partial(near_kernel, log_length=log_length), (state_sds, t...  3.42 us
    ppermute x1, starting transfers between devices, whole(): other = lax.ppermute(payload, 'sp', swap(sp, bits[0]))  2.66 us
  transfers between devices with their start and end apart: 13, of which 8 were waited for; matrix products, arithmetic and copies ran while one was open for 0% of the time, Pallas kernels for 15%

commit v1 on v0

--- a/solution.py
+++ b/solution.py
@@ -13,7 +13,7 @@
 DV = 128
 DECAY_TAU = 16.0
 ROW_PARTS = (2, 3, 3)
-COL_PARTS = (3, 1)
+COL_PARTS = (5, 3)
 LATE = len(COL_PARTS)
 VMEM_LIMIT = 8 * 1024 * 1024
 
@@ -150,11 +150,19 @@
         copy.wait()
 
 
-def near_kernel(x0, x1, wk, wv, wd, off, s_out, l_out, *, log_length):
+def near_kernel(x0, x1, *refs, log_length):
+    stored, off, kept, (s_out, l_out, sems) = refs[:3], refs[3], refs[4:7], refs[7:]
+    loads = [pltpu.make_async_copy(h, v, sems.at[n]) for n, (h, v) in enumerate(zip(stored, kept))]
+    for load in loads:
+        load.start()
     core = lax.rem(lax.axis_index("tp"), 2)
     rows = x0.shape[0]
     x = jnp.concatenate([x0[...], x1[...]], axis=0)
-    keys, values, log_decay = project(products(x, (wk, wv, wd)), off[...], log_length)
+    sums = []
+    for load, w in zip(loads, kept):
+        load.wait()
+        sums += products(x, [w])
+    keys, values, log_decay = project(sums, off[...], log_length)
     after = later_within(log_decay, [rows, rows])
     own = after[0:1] + log_decay[0:1]
     sib = after[rows : rows + 1] + log_decay[rows : rows + 1]
@@ -258,7 +266,7 @@
     pack(out, state, total, against(asked[...], state)[:heads] if last else None)
 
 
-def final_kernel(asked, mine, other, exact, cache, read, *, bit):
+def final_kernel(asked, mine, other, exact, cache_h, read_h, cache, read, sems, *, bit):
     heads, kept, _ = cache.shape
     key_cols = asked.shape[1]
     earlier = lax.bitwise_and(lax.axis_index("sp"), bit) == 0
@@ -277,21 +285,27 @@
     result = against(chosen, state)
     for h in range(heads):
         cache[h] = result[h * kept : (h + 1) * kept].astype(BF16)
+    send = pltpu.make_async_copy(cache, cache_h, sems.at[0])
+    send.start()
     heard = against(asked[...], first)[:heads]
     heard = heard + heard_of(jnp.where(earlier, tail_o, tail_m), heads)
     mean = jnp.mean(heard * heard, axis=-1, keepdims=True)
     read[...] = (heard * lax.rsqrt(mean + 1.0)).astype(BF16)
+    last = pltpu.make_async_copy(read, read_h, sems.at[1])
+    last.start()
+    send.wait()
+    last.wait()
 
 
 VM = pl.BlockSpec(memory_space=pltpu.VMEM)
 
 
-def call(kernel, out_shape, in_specs, scratch=(), flops=0):
+def call(kernel, out_shape, in_specs, scratch=(), flops=0, out_space=pltpu.VMEM):
     return pl.pallas_call(
         kernel,
         out_shape=out_shape,
         in_specs=in_specs,
-        out_specs=jax.tree.map(lambda _: VM, out_shape),
+        out_specs=jax.tree.map(lambda _: pl.BlockSpec(memory_space=out_space), out_shape),
         scratch_shapes=list(scratch),
         cost_estimate=pl.CostEstimate(flops=flops, bytes_accessed=0, transcendentals=0),
         compiler_params=pltpu.CompilerParams(vmem_limit_bytes=VMEM_LIMIT),
@@ -328,12 +342,15 @@
             far[bit, part] = lax.ppermute(piece, "tp", swap(tp, 2 * bit))
     sibling = lax.ppermute(tokens, "tp", swap(tp, 1))
 
-    s_near, l_near = call(
+    hbm = pl.BlockSpec(memory_space=pltpu.HBM)
+    weights = [pltpu.with_memory_space_constraint(w, pltpu.HBM) for w in (wk, wv, wd)]
+    wk, wv, wd, s_near, l_near = call(
         functools.partial(near_kernel, log_length=log_length),
-        (state_sds, total_sds),
-        [VM] * 6,
+        tuple(pltpu.VMEM(w.shape, BF16) for w in weights) + (state_sds, total_sds),
+        [VM, VM, hbm, hbm, hbm, VM],
+        [pltpu.SemaphoreType.DMA((3,))],
         flops=4 * rows * width * cols,
-    )(tokens, sibling, wk, wv, wd, offset)
+    )(tokens, sibling, *weights, offset)
 
     asked = call(ask_kernel, sds((heads + -heads % 8, key_cols), F32), [VM])(fresh_question)
 
@@ -391,10 +408,13 @@
             [VM] * (2 + len(others)),
         )(asked, payload, *others)
     other = lax.ppermute(payload, "sp", swap(sp, bits[0]))
+    outs = (sds((heads, CUE_WIDTH // sp, DV), BF16), sds((heads, DV), BF16))
     return call(
         functools.partial(final_kernel, bit=bits[0]),
-        (sds((heads, CUE_WIDTH // sp, DV), BF16), sds((heads, DV), BF16)),
+        outs,
         [VM] * 4,
+        [pltpu.VMEM(o.shape, o.dtype) for o in outs] + [pltpu.SemaphoreType.DMA((2,))],
+        out_space=pltpu.HBM,
     )(asked, payload, other, exact)
 
 

time: 61.6 us -> 56.5 us (0.917)
  local copies, waits for them, and re-layouts: 4.82 us -> 0.02 us
  Pallas kernels: 11.5 us -> 14.4 us
  starting transfers between devices: 13.3 us -> 11.6 us
  waiting for transfers between devices: 31 us -> 29.6 us
    unnamed x16 -> x6, local copies, waits for them, and re-layouts: 4.82 us -> 0.02 us
    pallas_call x2, Pallas kernels: 4.43 us -> 7.28 us  [the longest x1 6.25 us: whole(): call(functools.partial(near_kernel, log_length=log_length), tuple((pltpu....]
    ppermute x4, starting transfers between devices: 6.49 us -> 4.83 us  [whole(): far[bit, part] = lax.ppermute(piece, 'tp', swap(tp, 2 * bit))]
    ppermute x4, waiting for transfers between devices: 22 us -> 20.6 us  [whole(): far[bit, part] = lax.ppermute(piece, 'tp', swap(tp, 2 * bit))]
  transfers between devices with their start and end apart: 13 -> 13, of which waited for: 8 -> 8; matrix products, arithmetic and copies ran while one was open for 0% -> 0% of each run, Pallas kernels for 15% -> 21%
where the time goes in v1:
time: 56.5 us; the launch traced here: 56.4 us
  waiting for transfers between devices  29.6 us (52%)
  Pallas kernels  14.4 us (25%)
  starting transfers between devices  11.6 us (21%)
  between operations  0.76 us (1%)
    ppermute x4, waiting for transfers between devices, whole(): far[bit, part] = lax.ppermute(piece, 'tp', swap(tp, 2 * bit))  20.6 us
    pallas_call x1, Pallas kernels, whole(): call(functools.partial(near_kernel, log_length=log_length), tuple((pltpu....  6.25 us
    ppermute x3, waiting for transfers between devices, whole(): others.append(lax.ppermute(payload, 'sp', swap(sp, far_bits)))  5.02 us
    ppermute x4, starting transfers between devices, whole(): far[bit, part] = lax.ppermute(piece, 'tp', swap(tp, 2 * bit))  4.83 us
    ppermute x1, waiting for transfers between devices, whole(): other = lax.ppermute(payload, 'sp', swap(sp, bits[0]))  3.95 us
    ppermute x3, starting transfers between devices, whole(): others.append(lax.ppermute(payload, 'sp', swap(sp, far_bits)))  3.55 us
    ppermute x1, starting transfers between devices, whole(): other = lax.ppermute(payload, 'sp', swap(sp, bits[0]))  2.65 us
    pallas_call x1, Pallas kernels, whole(): call(functools.partial(early_kernel, log_length=log_length, pieces=len(ta...  2.39 us
  transfers between devices with their start and end apart: 13, of which 8 were waited for; matrix products, arithmetic and copies ran while one was open for 0% of the time, Pallas kernels for 21%

profile of v1, /device:TPU:0, one launch (start us, length us, event | category | flops | bytes accessed | tf_op | source)
XLA Modules:
  0.0 56.4 jit_solution(1829448462696939344)
XLA Ops:
  0.6 0.0 copy-start
  0.7 0.6 collective-permute-start.4
  1.2 1.2 %shard_map.78 = (bf16[48,4096]{1,0:T(8,128)(2,1)S(1)}, bf16[48,2560]{1,0:T(8,128)(2,1)S(1)}, bf16[48,1536]{1,0:T(8,128)(2,1)S(1)}) custom-call(bf16[128,4096]{1,0:T(8,128)(2,1)} %tokens.3), custom_call_target="tpu_custom_call" | custom-call | tf_op jit(solution)/shard_map/pallas_call | solution.py:333
  2.4 2.7 %collective-permute-start.6 = (bf16[48,4096]{1,0:T(8,128)(2,1)S(1)}, bf16[48,4096]{1,0:T(8,128)(2,1)S(1)}, u32[]{:S(2)}, u32[]{:S(2)}) collective-permute-start(bf16[48,4096]{1,0:T(8,128)(2,1)S(1)} %get-tuple-element.28), channel_id=1, source_target_pairs={{0,2},{1,3},{2,0},{3,1},{4,6},{5,7},{6,4},{7,5},{8,10},{9,11},{10,... | collective-permute-start | bytes 1179656 | tf_op jit(solution)/shard_map/ppermute | solution.py:342
  5.0 0.1 collective-permute-start.2
  5.1 1.0 %shard_map.81 = bf16[32,4096]{1,0:T(8,128)(2,1)S(1)} custom-call(bf16[128,4096]{1,0:T(8,128)(2,1)} %tokens.3), custom_call_target="tpu_custom_call" | custom-call | tf_op jit(solution)/shard_map/pallas_call | solution.py:333
  6.1 2.0 %collective-permute-start.5 = (bf16[32,4096]{1,0:T(8,128)(2,1)S(1)}, bf16[32,4096]{1,0:T(8,128)(2,1)S(1)}, u32[]{:S(2)}, u32[]{:S(2)}) collective-permute-start(bf16[32,4096]{1,0:T(8,128)(2,1)S(1)} %shard_map.81), channel_id=1, source_target_pairs={{0,2},{1,3},{2,0},{3,1},{4,6},{5,7},{6,4},{7,5},{8,10},{9,11},{10,... | collective-permute-start | bytes 786440 | tf_op jit(solution)/shard_map/ppermute | solution.py:342
  8.1 0.1 collective-permute-start
  8.2 6.8 %collective-permute-done.6.refs_1_ = bf16[48,4096]{1,0:T(8,128)(2,1)S(1)} collective-permute-done((bf16[48,4096]{1,0:T(8,128)(2,1)S(1)}, bf16[48,4096]{1,0:T(8,128)(2,1)S(1)}, u32[]{:S(2)}, u32[]{:S(2)}) %collective-permute-start.6) | collective-permute-done | bytes 393248 | tf_op jit(solution)/shard_map/ppermute | solution.py:342
  15.0 5.3 %collective-permute-done.2.xa = bf16[48,2560]{1,0:T(8,128)(2,1)S(1)} collective-permute-done((bf16[48,2560]{1,0:T(8,128)(2,1)S(1)}, bf16[48,2560]{1,0:T(8,128)(2,1)S(1)}, u32[]{:S(2)}, u32[]{:S(2)}) %collective-permute-start.2) | collective-permute-done | bytes 245792 | tf_op jit(solution)/shard_map/ppermute | solution.py:342
  20.3 0.0 collective-permute-start.3
  20.3 5.6 %collective-permute-done.5.refs_0_ = bf16[32,4096]{1,0:T(8,128)(2,1)S(1)} collective-permute-done((bf16[32,4096]{1,0:T(8,128)(2,1)S(1)}, bf16[32,4096]{1,0:T(8,128)(2,1)S(1)}, u32[]{:S(2)}, u32[]{:S(2)}) %collective-permute-start.5) | collective-permute-done | bytes 262176 | tf_op jit(solution)/shard_map/ppermute | solution.py:342
  25.9 0.0 collective-permute-start.7
  25.9 2.9 %collective-permute-done.xa = bf16[48,1536]{1,0:T(8,128)(2,1)S(1)} collective-permute-done((bf16[48,1536]{1,0:T(8,128)(2,1)S(1)}, bf16[48,1536]{1,0:T(8,128)(2,1)S(1)}, u32[]{:S(2)}, u32[]{:S(2)}) %collective-permute-start) | collective-permute-done | bytes 147488 | tf_op jit(solution)/shard_map/ppermute | solution.py:342
  28.8 0.0 collective-permute-start.1
  28.8 0.0 collective-permute-done.4.x1
  28.8 6.2 %shard_map.79 = (bf16[4096,256]{1,0:T(8,128)(2,1)S(1)}, bf16[4096,512]{1,0:T(8,128)(2,1)S(1)}, bf16[4096,256]{1,0:T(8,128)(2,1)S(1)}, f32[128,256]{1,0:T(8,128)S(1)}, f32[1,256]{1,0:T(1,128)S(1)}) custom-call(bf16[128,4096]{1,0:T(8,128)(2,1)S(1)} %copy-done, bf16[128,4096]{1,0:T(8,128)(2,1)S(1)} %collective-permute-done.4.x1, bf16[4096,256]{1,0:T(8,128)(2,1)} %refs_0_.1, ...), custom_call_target="tpu_custom_call" | custom-call | flops 2147483648 | tf_op jit(solution)/shard_map/pallas_call | solution.py:347
  35.1 1.0 %shard_map.80 = (f32[96,256]{1,0:T(8,128)S(1)}, f32[96,512]{1,0:T(8,128)S(1)}, f32[96,256]{1,0:T(8,128)S(1)}) custom-call(bf16[48,2560]{1,0:T(8,128)(2,1)S(1)} %collective-permute-done.2.xa, bf16[48,2560]{1,0:T(8,128)(2,1)S(1)} %collective-permute-done.3.xb, bf16[4096,256]{1,0:T(8,128)(2,1)S(1)} %get-tuple-element.21.wk.refs_4_, ...), custom_call_target="tpu_custom_call" | custom-call | flops 503316480 | tf_op jit(solution)/shard_map/pallas_call | solution.py:382
  36.1 2.4 %shard_map.82 = (f32[128,256]{1,0:T(8,128)S(1)}, f32[128,256]{1,0:T(8,128)S(1)}, f32[1,256]{1,0:T(1,128)S(1)}, f32[1,256]{1,0:T(1,128)S(1)}) custom-call(bf16[32,4096]{1,0:T(8,128)(2,1)S(1)} %collective-permute-done.5.refs_0_, bf16[48,4096]{1,0:T(8,128)(2,1)S(1)} %collective-permute-done.6.refs_1_, bf16[32,4096]{1,0:T(8,128)(2,1)S(1)} %collective-permute-done.7.refs_2_, ...), custom_call_target="tpu_custom_call" | custom-call | flops 1342177280 | tf_op jit(solution)/shard_map/pallas_call | solution.py:367
  38.5 0.0 copy-start.2
  38.5 1.2 %shard_map.83.refs_0_ = bf16[136,256]{1,0:T(8,128)(2,1)S(1)} custom-call(bf16[48,1536]{1,0:T(8,128)(2,1)S(1)} %collective-permute-done.xa, bf16[48,1536]{1,0:T(8,128)(2,1)S(1)} %collective-permute-done.1.xb, f32[96,256]{1,0:T(8,128)S(1)} %get-tuple-element.24.ks, f32[96,512]{1,0:T(8,128)S(1)} %get-tuple-element.25.vs, f32[96,256]{1,0:T(8,128)S(1)} %get-tuple-element.26.ds, ...), custom_call_target="tpu_custom_call" | custom-call | flops 301989888 | tf_op jit(solution)/shard_map/pallas_call | solution.py:388
  39.7 1.9 %collective-permute-start.10 = (bf16[136,256]{1,0:T(8,128)(2,1)S(1)}, bf16[136,256]{1,0:T(8,128)(2,1)S(1)}, u32[]{:S(2)}, u32[]{:S(2)}) collective-permute-start(bf16[136,256]{1,0:T(8,128)(2,1)S(1)} %shard_map.83.refs_0_), channel_id=1, source_target_pairs={{0,8},{4,12},{8,0},{12,4},{16,24},{20,28},{24,16},{28,20},{1,9},{5... | collective-permute-start | bytes 208904 | tf_op jit(solution)/shard_map/ppermute | solution.py:404
  41.6 1.4 %collective-permute-start.11 = (bf16[136,256]{1,0:T(8,128)(2,1)S(1)}, bf16[136,256]{1,0:T(8,128)(2,1)S(1)}, u32[]{:S(2)}, u32[]{:S(2)}) collective-permute-start(bf16[136,256]{1,0:T(8,128)(2,1)S(1)} %shard_map.83.refs_0_), channel_id=1, source_target_pairs={{0,12},{4,8},{8,4},{12,0},{16,28},{20,24},{24,20},{28,16},{1,13},{... | collective-permute-start | bytes 208904 | tf_op jit(solution)/shard_map/ppermute | solution.py:404
  43.0 0.3 collective-permute-start.9
  43.3 0.1 shard_map.77.asked
  43.4 1.1 %collective-permute-done.10.refs_2_ = bf16[136,256]{1,0:T(8,128)(2,1)S(1)} collective-permute-done((bf16[136,256]{1,0:T(8,128)(2,1)S(1)}, bf16[136,256]{1,0:T(8,128)(2,1)S(1)}, u32[]{:S(2)}, u32[]{:S(2)}) %collective-permute-start.10) | collective-permute-done | bytes 69664 | tf_op jit(solution)/shard_map/ppermute | solution.py:404
  44.5 2.7 %collective-permute-done.11.refs_3_ = bf16[136,256]{1,0:T(8,128)(2,1)S(1)} collective-permute-done((bf16[136,256]{1,0:T(8,128)(2,1)S(1)}, bf16[136,256]{1,0:T(8,128)(2,1)S(1)}, u32[]{:S(2)}, u32[]{:S(2)}) %collective-permute-start.11) | collective-permute-done | bytes 69664 | tf_op jit(solution)/shard_map/ppermute | solution.py:404
  47.1 1.3 %collective-permute-done.9.refs_1_ = bf16[136,256]{1,0:T(8,128)(2,1)S(1)} collective-permute-done((bf16[136,256]{1,0:T(8,128)(2,1)S(1)}, bf16[136,256]{1,0:T(8,128)(2,1)S(1)}, u32[]{:S(2)}, u32[]{:S(2)}) %collective-permute-start.9) | collective-permute-done | bytes 69664 | tf_op jit(solution)/shard_map/ppermute | solution.py:404
  48.4 0.3 shard_map.84
  48.7 2.7 %collective-permute-start.12 = (bf16[144,256]{1,0:T(8,128)(2,1)S(1)}, bf16[144,256]{1,0:T(8,128)(2,1)S(1)}, u32[]{:S(2)}, u32[]{:S(2)}) collective-permute-start(bf16[144,256]{1,0:T(8,128)(2,1)S(1)} %get-tuple-element.34.mine), channel_id=1, source_target_pairs={{0,16},{4,20},{8,24},{12,28},{16,0},{20,4},{24,8},{28,12},{1,17},{... | collective-permute-start | bytes 221192 | tf_op jit(solution)/shard_map/ppermute | solution.py:410
  51.4 4.0 %collective-permute-done.12.other = bf16[144,256]{1,0:T(8,128)(2,1)S(1)} collective-permute-done((bf16[144,256]{1,0:T(8,128)(2,1)S(1)}, bf16[144,256]{1,0:T(8,128)(2,1)S(1)}, u32[]{:S(2)}, u32[]{:S(2)}) %collective-permute-start.12) | collective-permute-done | bytes 73760 | tf_op jit(solution)/shard_map/ppermute | solution.py:410
  55.3 1.0 %shard_map.85 = (bf16[4,8,128]{2,1,0:T(8,128)(2,1)}, bf16[4,128]{1,0:T(4,128)(2,1)}) custom-call(f32[8,256]{1,0:T(8,128)S(1)} %shard_map.77.asked, bf16[144,256]{1,0:T(8,128)(2,1)S(1)} %get-tuple-element.34.mine, bf16[144,256]{1,0:T(8,128)(2,1)S(1)} %collective-permute-done.12.other, f32[128,256]{1,0:T(8,128)S(1)} %get-tuple-element.35.exact), custom_call_target="tpu_custom_call" | custom-call | tf_op jit(solution)/shard_map/pallas_call | solution.py:412
  (9 shorter events, 0.0 us)
Async XLA Ops:
  0.6 28.2 %copy-start = (bf16[128,4096]{1,0:T(8,128)(2,1)S(1)}, bf16[128,4096]{1,0:T(8,128)(2,1)}, u32[]{:S(2)}) copy-start(bf16[128,4096]{1,0:T(8,128)(2,1)} %tokens.3) | copy-start | bytes 3145732
  0.6 28.2 %copy-start.1 = (f32[256]{0:T(256)S(1)}, f32[256]{0:T(256)}, u32[]{:S(2)}) copy-start(f32[256]{0:T(256)} %param.10) | copy-start | bytes 3076
  0.7 28.1 %collective-permute-start.4 = (bf16[128,4096]{1,0:T(8,128)(2,1)}, bf16[128,4096]{1,0:T(8,128)(2,1)S(1)}, u32[]{:S(2)}, u32[]{:S(2)}) collective-permute-start(bf16[128,4096]{1,0:T(8,128)(2,1)} %tokens.3), channel_id=1, source_target_pairs={{0,1},{1,0},{2,3},{3,2},{4,5},{5,4},{6,7},{7,6},{8,9},{9,8},{10,11... | collective-permute-start | bytes 3145736 | tf_op jit(solution)/shard_map/ppermute | solution.py:343
  2.4 12.6 %collective-permute-start.6 = (bf16[48,4096]{1,0:T(8,128)(2,1)S(1)}, bf16[48,4096]{1,0:T(8,128)(2,1)S(1)}, u32[]{:S(2)}, u32[]{:S(2)}) collective-permute-start(bf16[48,4096]{1,0:T(8,128)(2,1)S(1)} %get-tuple-element.28), channel_id=1, source_target_pairs={{0,2},{1,3},{2,0},{3,1},{4,6},{5,7},{6,4},{7,5},{8,10},{9,11},{10,... | collective-permute-start | bytes 1179656 | tf_op jit(solution)/shard_map/ppermute | solution.py:342
  5.0 15.2 %collective-permute-start.2 = (bf16[48,2560]{1,0:T(8,128)(2,1)S(1)}, bf16[48,2560]{1,0:T(8,128)(2,1)S(1)}, u32[]{:S(2)}, u32[]{:S(2)}) collective-permute-start(bf16[48,2560]{1,0:T(8,128)(2,1)S(1)} %get-tuple-element.20), channel_id=1, source_target_pairs={{0,2},{1,3},{2,0},{3,1},{4,6},{5,7},{6,4},{7,5},{8,10},{9,11},{10,... | collective-permute-start | bytes 737288 | tf_op jit(solution)/shard_map/ppermute | solution.py:342
  6.1 19.8 %collective-permute-start.5 = (bf16[32,4096]{1,0:T(8,128)(2,1)S(1)}, bf16[32,4096]{1,0:T(8,128)(2,1)S(1)}, u32[]{:S(2)}, u32[]{:S(2)}) collective-permute-start(bf16[32,4096]{1,0:T(8,128)(2,1)S(1)} %shard_map.81), channel_id=1, source_target_pairs={{0,2},{1,3},{2,0},{3,1},{4,6},{5,7},{6,4},{7,5},{8,10},{9,11},{10,... | collective-permute-start | bytes 786440 | tf_op jit(solution)/shard_map/ppermute | solution.py:342
  8.1 20.7 %collective-permute-start = (bf16[48,1536]{1,0:T(8,128)(2,1)S(1)}, bf16[48,1536]{1,0:T(8,128)(2,1)S(1)}, u32[]{:S(2)}, u32[]{:S(2)}) collective-permute-start(bf16[48,1536]{1,0:T(8,128)(2,1)S(1)} %get-tuple-element.19), channel_id=1, source_target_pairs={{0,2},{1,3},{2,0},{3,1},{4,6},{5,7},{6,4},{7,5},{8,10},{9,11},{10,... | collective-permute-start | bytes 442376 | tf_op jit(solution)/shard_map/ppermute | solution.py:342
  15.0 21.1 %collective-permute-start.8 = (bf16[48,4096]{1,0:T(8,128)(2,1)S(1)}, bf16[48,4096]{1,0:T(8,128)(2,1)S(1)}, u32[]{:S(2)}, u32[]{:S(2)}) collective-permute-start(bf16[48,4096]{1,0:T(8,128)(2,1)S(1)} %collective-permute-done.6.refs_1_), channel_id=1, source_target_pairs={{0,1},{1,0},{2,3},{3,2},{4,5},{5,4},{6,7},{7,6},{8,9},{9,8},{10,11... | collective-permute-start | bytes 1179656 | tf_op jit(solution)/shard_map/ppermute | solution.py:360
  20.3 14.8 %collective-permute-start.3 = (bf16[48,2560]{1,0:T(8,128)(2,1)S(1)}, bf16[48,2560]{1,0:T(8,128)(2,1)S(1)}, u32[]{:S(2)}, u32[]{:S(2)}) collective-permute-start(bf16[48,2560]{1,0:T(8,128)(2,1)S(1)} %collective-permute-done.2.xa), channel_id=1, source_target_pairs={{0,1},{1,0},{2,3},{3,2},{4,5},{5,4},{6,7},{7,6},{8,9},{9,8},{10,11... | collective-permute-start | bytes 737288 | tf_op jit(solution)/shard_map/ppermute | solution.py:360
  25.9 10.2 %collective-permute-start.7 = (bf16[32,4096]{1,0:T(8,128)(2,1)S(1)}, bf16[32,4096]{1,0:T(8,128)(2,1)S(1)}, u32[]{:S(2)}, u32[]{:S(2)}) collective-permute-start(bf16[32,4096]{1,0:T(8,128)(2,1)S(1)} %collective-permute-done.5.refs_0_), channel_id=1, source_target_pairs={{0,1},{1,0},{2,3},{3,2},{4,5},{5,4},{6,7},{7,6},{8,9},{9,8},{10,11... | collective-permute-start | bytes 786440 | tf_op jit(solution)/shard_map/ppermute | solution.py:360
  28.8 9.7 %collective-permute-start.1 = (bf16[48,1536]{1,0:T(8,128)(2,1)S(1)}, bf16[48,1536]{1,0:T(8,128)(2,1)S(1)}, u32[]{:S(2)}, u32[]{:S(2)}) collective-permute-start(bf16[48,1536]{1,0:T(8,128)(2,1)S(1)} %collective-permute-done.xa), channel_id=1, source_target_pairs={{0,1},{1,0},{2,3},{3,2},{4,5},{5,4},{6,7},{7,6},{8,9},{9,8},{10,11... | collective-permute-start | bytes 442376 | tf_op jit(solution)/shard_map/ppermute | solution.py:360
  38.5 4.8 %copy-start.2 = (bf16[4,64]{1,0:T(4,128)(2,1)S(1)}, bf16[4,64]{1,0:T(4,128)(2,1)}, u32[]{:S(2)}) copy-start(bf16[4,64]{1,0:T(4,128)(2,1)} %question.1) | copy-start | bytes 1540
  39.7 4.7 %collective-permute-start.10 = (bf16[136,256]{1,0:T(8,128)(2,1)S(1)}, bf16[136,256]{1,0:T(8,128)(2,1)S(1)}, u32[]{:S(2)}, u32[]{:S(2)}) collective-permute-start(bf16[136,256]{1,0:T(8,128)(2,1)S(1)} %shard_map.83.refs_0_), channel_id=1, source_target_pairs={{0,8},{4,12},{8,0},{12,4},{16,24},{20,28},{24,16},{28,20},{1,9},{5... | collective-permute-start | bytes 208904 | tf_op jit(solution)/shard_map/ppermute | solution.py:404
  41.6 5.5 %collective-permute-start.11 = (bf16[136,256]{1,0:T(8,128)(2,1)S(1)}, bf16[136,256]{1,0:T(8,128)(2,1)S(1)}, u32[]{:S(2)}, u32[]{:S(2)}) collective-permute-start(bf16[136,256]{1,0:T(8,128)(2,1)S(1)} %shard_map.83.refs_0_), channel_id=1, source_target_pairs={{0,12},{4,8},{8,4},{12,0},{16,28},{20,24},{24,20},{28,16},{1,13},{... | collective-permute-start | bytes 208904 | tf_op jit(solution)/shard_map/ppermute | solution.py:404
  43.0 5.4 %collective-permute-start.9 = (bf16[136,256]{1,0:T(8,128)(2,1)S(1)}, bf16[136,256]{1,0:T(8,128)(2,1)S(1)}, u32[]{:S(2)}, u32[]{:S(2)}) collective-permute-start(bf16[136,256]{1,0:T(8,128)(2,1)S(1)} %shard_map.83.refs_0_), channel_id=1, source_target_pairs={{0,4},{4,0},{8,12},{12,8},{16,20},{20,16},{24,28},{28,24},{1,5},{5... | collective-permute-start | bytes 208904 | tf_op jit(solution)/shard_map/ppermute | solution.py:404
  48.7 6.6 %collective-permute-start.12 = (bf16[144,256]{1,0:T(8,128)(2,1)S(1)}, bf16[144,256]{1,0:T(8,128)(2,1)S(1)}, u32[]{:S(2)}, u32[]{:S(2)}) collective-permute-start(bf16[144,256]{1,0:T(8,128)(2,1)S(1)} %get-tuple-element.34.mine), channel_id=1, source_target_pairs={{0,16},{4,20},{8,24},{12,28},{16,0},{20,4},{24,8},{28,12},{1,17},{... | collective-permute-start | bytes 221192 | tf_op jit(solution)/shard_map/ppermute | solution.py:410

commit v2 on v1

--- a/solution.py
+++ b/solution.py
@@ -13,7 +13,7 @@
 DV = 128
 DECAY_TAU = 16.0
 ROW_PARTS = (2, 3, 3)
-COL_PARTS = (5, 3)
+COL_PARTS = (8, 5, 3)
 LATE = len(COL_PARTS)
 VMEM_LIMIT = 8 * 1024 * 1024
 
@@ -48,7 +48,10 @@
     for size in sizes[:-1]:
         edge += size
         mask = mask & ((i >= edge) == (j >= edge))
-    return jnp.dot(mask.astype(F32), log_decay, precision=EXACT, preferred_element_type=F32)
+    parts = jnp.concatenate([p.astype(BF16) for p in split(log_decay)], axis=1)
+    sums = jnp.dot(mask.astype(BF16), parts, preferred_element_type=F32)
+    cols = log_decay.shape[1]
+    return sums[:, :cols] + sums[:, cols : 2 * cols] + sums[:, 2 * cols :]
 
 
 def weigh(keys, after):
@@ -193,10 +196,11 @@
     l_b[...] = after[rows : rows + 1] + log_decay[rows : rows + 1]
 
 
-def partial_kernel(xa, xb, wk, wv, wd, *outs):
+def partial_kernel(xa, xb, wk, wv, wd, *refs, start):
     x = jnp.concatenate([xa[...], xb[...]], axis=0)
-    for out, value in zip(outs, products(x, (wk, wv, wd))):
-        out[...] = value
+    outs = refs[-3:]
+    for n, value in enumerate(products(x, (wk, wv, wd), start)):
+        outs[n][...] = refs[n][...] + value if start else value
 
 
 def late_kernel(xa, xb, ks, vs, ds, wk, wv, wd, off, *refs, log_length, blocks, here, parts):
@@ -379,20 +383,22 @@
         states += [s_a, s_b]
         totals += [l_a, l_b]
     late_rows = 2 * (edges[-1] - edges[-2])
-    sums = call(
-        partial_kernel,
-        tuple(sds((late_rows, w.shape[1]), F32) for w in (wk, wv, wd)),
-        [VM] * 5,
-        flops=2 * late_rows * sides[1] * cols,
-    )(*last[0], wk, wv, wd)
+    sums = []
+    for n in range(LATE - 1):
+        sums = call(
+            functools.partial(partial_kernel, start=sides[n]),
+            tuple(sds((late_rows, w.shape[1]), F32) for w in (wk, wv, wd)),
+            [VM] * (5 + len(sums)),
+            flops=2 * late_rows * (sides[n + 1] - sides[n]) * cols,
+        )(*last[n], wk, wv, wd, *sums)
     payload = call(
         functools.partial(
             late_kernel, log_length=log_length, blocks=tuple(blocks), here=(final_bit, 1), parts=2
         ),
         payload_sds(heads, sp == 2),
         [VM] * (9 + 2 * len(blocks)),
-        flops=2 * late_rows * (width - sides[1]) * cols,
-    )(*last[1], *sums, wk, wv, wd, offset, *states, *totals)
+        flops=2 * late_rows * (width - sides[-2]) * cols,
+    )(*last[-1], *sums, wk, wv, wd, offset, *states, *totals)
 
     bits = [1 << n for n in range(sp.bit_length() - 1)]
     while len(bits) > 1:

time: 56.5 us -> 56.1 us (level)
  waiting for transfers between devices: 29.6 us -> 27 us
  starting transfers between devices: 11.6 us -> 14.2 us
    ppermute x4 -> x5, starting transfers between devices: 4.83 us -> 6.84 us  [whole(): far[bit, part] = lax.ppermute(piece, 'tp', swap(tp, 2 * bit))]
    ppermute x4 -> x5, waiting for transfers between devices: 20.6 us -> 18.6 us  [whole(): far[bit, part] = lax.ppermute(piece, 'tp', swap(tp, 2 * bit))]
    ppermute x4 -> x5, starting transfers between devices: 0.01 us -> 0.59 us  [whole(): lax.ppermute(far[bit, part], 'tp', swap(tp, 1))]
    pallas_call x1 -> x2, Pallas kernels: 0.98 us -> 1.37 us  [whole(): call(functools.partial(partial_kernel, start=sides[n]), tuple((sds((late_...]
  transfers between devices with their start and end apart: 13 -> 15, of which waited for: 8 -> 7; matrix products, arithmetic and copies ran while one was open for 0% -> 0% of each run, Pallas kernels for 21% -> 21%
where the time goes in v2:
time: 56.1 us; the launch traced here: 56 us
  waiting for transfers between devices  27 us (48%)
  starting transfers between devices  14.2 us (25%)
  Pallas kernels  14 us (25%)
  between operations  0.76 us (1%)
    ppermute x5, waiting for transfers between devices, whole(): far[bit, part] = lax.ppermute(piece, 'tp', swap(tp, 2 * bit))  18.6 us
    ppermute x5, starting transfers between devices, whole(): far[bit, part] = lax.ppermute(piece, 'tp', swap(tp, 2 * bit))  6.84 us
    pallas_call x1, Pallas kernels, whole(): call(functools.partial(near_kernel, log_length=log_length), tuple((pltpu....  6.03 us
    ppermute x3, waiting for transfers between devices, whole(): others.append(lax.ppermute(payload, 'sp', swap(sp, far_bits)))  4.94 us
    ppermute x3, starting transfers between devices, whole(): others.append(lax.ppermute(payload, 'sp', swap(sp, far_bits)))  3.55 us
    ppermute x1, waiting for transfers between devices, whole(): other = lax.ppermute(payload, 'sp', swap(sp, bits[0]))  3.45 us
    ppermute x1, starting transfers between devices, whole(): other = lax.ppermute(payload, 'sp', swap(sp, bits[0]))  2.64 us
    pallas_call x1, Pallas kernels, whole(): call(functools.partial(early_kernel, log_length=log_length, pieces=len(ta...  2.19 us
  transfers between devices with their start and end apart: 15, of which 7 were waited for; matrix products, arithmetic and copies ran while one was open for 0% of the time, Pallas kernels for 21%

profile of v2, /device:TPU:0, one launch (start us, length us, event | category | flops | bytes accessed | tf_op | source)
XLA Modules:
  0.0 56.0 jit_solution(937147542565849808)
XLA Ops:
  0.6 0.0 copy-start
  0.7 0.6 collective-permute-start.4
  1.2 1.2 %shard_map.78 = (bf16[48,4096]{1,0:T(8,128)(2,1)S(1)}, bf16[48,2048]{1,0:T(8,128)(2,1)S(1)}, bf16[48,1280]{1,0:T(8,128)(2,1)S(1)}, bf16[48,768]{1,0:T(8,128)(2,1)S(1)}) custom-call(bf16[128,4096]{1,0:T(8,128)(2,1)} %tokens.3), custom_call_target="tpu_custom_call" | custom-call | tf_op jit(solution)/shard_map/pallas_call | solution.py:337
  2.4 2.7 %collective-permute-start.8 = (bf16[48,4096]{1,0:T(8,128)(2,1)S(1)}, bf16[48,4096]{1,0:T(8,128)(2,1)S(1)}, u32[]{:S(2)}, u32[]{:S(2)}) collective-permute-start(bf16[48,4096]{1,0:T(8,128)(2,1)S(1)} %get-tuple-element.36), channel_id=1, source_target_pairs={{0,2},{1,3},{2,0},{3,1},{4,6},{5,7},{6,4},{7,5},{8,10},{9,11},{10,... | collective-permute-start | bytes 1179656 | tf_op jit(solution)/shard_map/ppermute | solution.py:346
  5.0 1.0 %shard_map.82 = bf16[32,4096]{1,0:T(8,128)(2,1)S(1)} custom-call(bf16[128,4096]{1,0:T(8,128)(2,1)} %tokens.3), custom_call_target="tpu_custom_call" | custom-call | tf_op jit(solution)/shard_map/pallas_call | solution.py:337
  6.0 0.1 collective-permute-start.7
  6.1 2.0 %collective-permute-start = (bf16[48,768]{1,0:T(8,128)(2,1)S(1)}, bf16[48,768]{1,0:T(8,128)(2,1)S(1)}, u32[]{:S(2)}, u32[]{:S(2)}) collective-permute-start(bf16[48,768]{1,0:T(8,128)(2,1)S(1)} %get-tuple-element.23), channel_id=1, source_target_pairs={{0,2},{1,3},{2,0},{3,1},{4,6},{5,7},{6,4},{7,5},{8,10},{9,11},{10,... | collective-permute-start | bytes 221192 | tf_op jit(solution)/shard_map/ppermute | solution.py:346
  8.1 0.1 collective-permute-start.5
  8.2 6.8 %collective-permute-done.8.refs_1_ = bf16[48,4096]{1,0:T(8,128)(2,1)S(1)} collective-permute-done((bf16[48,4096]{1,0:T(8,128)(2,1)S(1)}, bf16[48,4096]{1,0:T(8,128)(2,1)S(1)}, u32[]{:S(2)}, u32[]{:S(2)}) %collective-permute-start.8) | collective-permute-done | bytes 393248 | tf_op jit(solution)/shard_map/ppermute | solution.py:346
  15.0 0.0 collective-permute-start.10
  15.0 7.2 %collective-permute-done.xa = bf16[48,768]{1,0:T(8,128)(2,1)S(1)} collective-permute-done((bf16[48,768]{1,0:T(8,128)(2,1)S(1)}, bf16[48,768]{1,0:T(8,128)(2,1)S(1)}, u32[]{:S(2)}, u32[]{:S(2)}) %collective-permute-start) | collective-permute-done | bytes 73760 | tf_op jit(solution)/shard_map/ppermute | solution.py:346
  22.2 2.0 %collective-permute-start.2 = (bf16[48,1280]{1,0:T(8,128)(2,1)S(1)}, bf16[48,1280]{1,0:T(8,128)(2,1)S(1)}, u32[]{:S(2)}, u32[]{:S(2)}) collective-permute-start(bf16[48,1280]{1,0:T(8,128)(2,1)S(1)} %get-tuple-element.24), channel_id=1, source_target_pairs={{0,2},{1,3},{2,0},{3,1},{4,6},{5,7},{6,4},{7,5},{8,10},{9,11},{10,... | collective-permute-start | bytes 368648 | tf_op jit(solution)/shard_map/ppermute | solution.py:346
  24.2 4.6 %collective-permute-done.2.xa = bf16[48,1280]{1,0:T(8,128)(2,1)S(1)} collective-permute-done((bf16[48,1280]{1,0:T(8,128)(2,1)S(1)}, bf16[48,1280]{1,0:T(8,128)(2,1)S(1)}, u32[]{:S(2)}, u32[]{:S(2)}) %collective-permute-start.2) | collective-permute-done | bytes 122912 | tf_op jit(solution)/shard_map/ppermute | solution.py:346
  28.8 0.5 collective-permute-start.3
  29.3 0.1 collective-permute-start.6
  29.4 6.0 %shard_map.79 = (bf16[4096,256]{1,0:T(8,128)(2,1)S(1)}, bf16[4096,512]{1,0:T(8,128)(2,1)S(1)}, bf16[4096,256]{1,0:T(8,128)(2,1)S(1)}, f32[128,256]{1,0:T(8,128)S(1)}, f32[1,256]{1,0:T(1,128)S(1)}) custom-call(bf16[128,4096]{1,0:T(8,128)(2,1)S(1)} %copy-done, bf16[128,4096]{1,0:T(8,128)(2,1)S(1)} %collective-permute-done.4.x1, bf16[4096,256]{1,0:T(8,128)(2,1)} %refs_0_.1, ...), custom_call_target="tpu_custom_call" | custom-call | flops 2147483648 | tf_op jit(solution)/shard_map/pallas_call | solution.py:351
  35.4 2.2 %shard_map.83 = (f32[128,256]{1,0:T(8,128)S(1)}, f32[128,256]{1,0:T(8,128)S(1)}, f32[1,256]{1,0:T(1,128)S(1)}, f32[1,256]{1,0:T(1,128)S(1)}) custom-call(bf16[32,4096]{1,0:T(8,128)(2,1)S(1)} %collective-permute-done.7.refs_0_, bf16[48,4096]{1,0:T(8,128)(2,1)S(1)} %collective-permute-done.8.refs_1_, bf16[32,4096]{1,0:T(8,128)(2,1)S(1)} %collective-permute-done.9.refs_2_, ...), custom_call_target="tpu_custom_call" | custom-call | flops 1342177280 | tf_op jit(solution)/shard_map/pallas_call | solution.py:371
  37.6 0.8 %shard_map.80 = (f32[96,256]{1,0:T(8,128)S(1)}, f32[96,512]{1,0:T(8,128)S(1)}, f32[96,256]{1,0:T(8,128)S(1)}) custom-call(bf16[48,2048]{1,0:T(8,128)(2,1)S(1)} %collective-permute-done.5.xa, bf16[48,2048]{1,0:T(8,128)(2,1)S(1)} %collective-permute-done.6.xb, bf16[4096,256]{1,0:T(8,128)(2,1)S(1)} %get-tuple-element.25.wk.refs_4_, ...), custom_call_target="tpu_custom_call" | custom-call | flops 402653184 | tf_op jit(solution)/shard_map/pallas_call | solution.py:388
  38.5 0.6 %shard_map.81 = (f32[96,256]{1,0:T(8,128)S(1)}, f32[96,512]{1,0:T(8,128)S(1)}, f32[96,256]{1,0:T(8,128)S(1)}) custom-call(bf16[48,1280]{1,0:T(8,128)(2,1)S(1)} %collective-permute-done.2.xa, bf16[48,1280]{1,0:T(8,128)(2,1)S(1)} %collective-permute-done.3.xb, bf16[4096,256]{1,0:T(8,128)(2,1)S(1)} %get-tuple-element.25.wk.refs_4_, ...), custom_call_target="tpu_custom_call" | custom-call | flops 251658240 | tf_op jit(solution)/shard_map/pallas_call | solution.py:388
  39.0 0.0 copy-start.2
  39.1 0.9 %shard_map.84.refs_0_ = bf16[136,256]{1,0:T(8,128)(2,1)S(1)} custom-call(bf16[48,768]{1,0:T(8,128)(2,1)S(1)} %collective-permute-done.xa, bf16[48,768]{1,0:T(8,128)(2,1)S(1)} %collective-permute-done.1.xb, f32[96,256]{1,0:T(8,128)S(1)} %get-tuple-element.32.ks, f32[96,512]{1,0:T(8,128)S(1)} %get-tuple-element.33.vs, f32[96,256]{1,0:T(8,128)S(1)} %get-tuple-element.34.ds, ...), custom_call_target="tpu_custom_call" | custom-call | flops 150994944 | tf_op jit(solution)/shard_map/pallas_call | solution.py:394
  39.9 1.8 %collective-permute-start.11 = (bf16[136,256]{1,0:T(8,128)(2,1)S(1)}, bf16[136,256]{1,0:T(8,128)(2,1)S(1)}, u32[]{:S(2)}, u32[]{:S(2)}) collective-permute-start(bf16[136,256]{1,0:T(8,128)(2,1)S(1)} %shard_map.84.refs_0_), channel_id=1, source_target_pairs={{0,4},{4,0},{8,12},{12,8},{16,20},{20,16},{24,28},{28,24},{1,5},{5... | collective-permute-start | bytes 208904 | tf_op jit(solution)/shard_map/ppermute | solution.py:410
  41.7 1.6 %collective-permute-start.12 = (bf16[136,256]{1,0:T(8,128)(2,1)S(1)}, bf16[136,256]{1,0:T(8,128)(2,1)S(1)}, u32[]{:S(2)}, u32[]{:S(2)}) collective-permute-start(bf16[136,256]{1,0:T(8,128)(2,1)S(1)} %shard_map.84.refs_0_), channel_id=1, source_target_pairs={{0,8},{4,12},{8,0},{12,4},{16,24},{20,28},{24,16},{28,20},{1,9},{5... | collective-permute-start | bytes 208904 | tf_op jit(solution)/shard_map/ppermute | solution.py:410
  43.3 0.2 collective-permute-start.13
  43.5 0.1 shard_map.77.asked
  43.6 1.0 %collective-permute-done.11.refs_1_ = bf16[136,256]{1,0:T(8,128)(2,1)S(1)} collective-permute-done((bf16[136,256]{1,0:T(8,128)(2,1)S(1)}, bf16[136,256]{1,0:T(8,128)(2,1)S(1)}, u32[]{:S(2)}, u32[]{:S(2)}) %collective-permute-start.11) | collective-permute-done | bytes 69664 | tf_op jit(solution)/shard_map/ppermute | solution.py:410
  44.5 1.8 %collective-permute-done.12.refs_2_ = bf16[136,256]{1,0:T(8,128)(2,1)S(1)} collective-permute-done((bf16[136,256]{1,0:T(8,128)(2,1)S(1)}, bf16[136,256]{1,0:T(8,128)(2,1)S(1)}, u32[]{:S(2)}, u32[]{:S(2)}) %collective-permute-start.12) | collective-permute-done | bytes 69664 | tf_op jit(solution)/shard_map/ppermute | solution.py:410
  46.3 2.2 %collective-permute-done.13.refs_3_ = bf16[136,256]{1,0:T(8,128)(2,1)S(1)} collective-permute-done((bf16[136,256]{1,0:T(8,128)(2,1)S(1)}, bf16[136,256]{1,0:T(8,128)(2,1)S(1)}, u32[]{:S(2)}, u32[]{:S(2)}) %collective-permute-start.13) | collective-permute-done | bytes 69664 | tf_op jit(solution)/shard_map/ppermute | solution.py:410
  48.5 0.3 shard_map.85
  48.8 2.6 %collective-permute-start.14 = (bf16[144,256]{1,0:T(8,128)(2,1)S(1)}, bf16[144,256]{1,0:T(8,128)(2,1)S(1)}, u32[]{:S(2)}, u32[]{:S(2)}) collective-permute-start(bf16[144,256]{1,0:T(8,128)(2,1)S(1)} %get-tuple-element.42.mine), channel_id=1, source_target_pairs={{0,16},{4,20},{8,24},{12,28},{16,0},{20,4},{24,8},{28,12},{1,17},{... | collective-permute-start | bytes 221192 | tf_op jit(solution)/shard_map/ppermute | solution.py:416
  51.5 3.5 %collective-permute-done.14.other = bf16[144,256]{1,0:T(8,128)(2,1)S(1)} collective-permute-done((bf16[144,256]{1,0:T(8,128)(2,1)S(1)}, bf16[144,256]{1,0:T(8,128)(2,1)S(1)}, u32[]{:S(2)}, u32[]{:S(2)}) %collective-permute-start.14) | collective-permute-done | bytes 73760 | tf_op jit(solution)/shard_map/ppermute | solution.py:416
  54.9 1.0 %shard_map.86 = (bf16[4,8,128]{2,1,0:T(8,128)(2,1)}, bf16[4,128]{1,0:T(4,128)(2,1)}) custom-call(f32[8,256]{1,0:T(8,128)S(1)} %shard_map.77.asked, bf16[144,256]{1,0:T(8,128)(2,1)S(1)} %get-tuple-element.42.mine, bf16[144,256]{1,0:T(8,128)(2,1)S(1)} %collective-permute-done.14.other, f32[128,256]{1,0:T(8,128)S(1)} %get-tuple-element.43.exact), custom_call_target="tpu_custom_call" | custom-call | tf_op jit(solution)/shard_map/pallas_call | solution.py:418
  (14 shorter events, 0.0 us)
Async XLA Ops:
  0.6 28.7 %copy-start = (bf16[128,4096]{1,0:T(8,128)(2,1)S(1)}, bf16[128,4096]{1,0:T(8,128)(2,1)}, u32[]{:S(2)}) copy-start(bf16[128,4096]{1,0:T(8,128)(2,1)} %tokens.3) | copy-start | bytes 3145732
  0.6 28.7 %copy-start.1 = (f32[256]{0:T(256)S(1)}, f32[256]{0:T(256)}, u32[]{:S(2)}) copy-start(f32[256]{0:T(256)} %param.10) | copy-start | bytes 3076
  0.7 28.7 %collective-permute-start.4 = (bf16[128,4096]{1,0:T(8,128)(2,1)}, bf16[128,4096]{1,0:T(8,128)(2,1)S(1)}, u32[]{:S(2)}, u32[]{:S(2)}) collective-permute-start(bf16[128,4096]{1,0:T(8,128)(2,1)} %tokens.3), channel_id=1, source_target_pairs={{0,1},{1,0},{2,3},{3,2},{4,5},{5,4},{6,7},{7,6},{8,9},{9,8},{10,11... | collective-permute-start | bytes 3145736 | tf_op jit(solution)/shard_map/ppermute | solution.py:347
  2.4 12.6 %collective-permute-start.8 = (bf16[48,4096]{1,0:T(8,128)(2,1)S(1)}, bf16[48,4096]{1,0:T(8,128)(2,1)S(1)}, u32[]{:S(2)}, u32[]{:S(2)}) collective-permute-start(bf16[48,4096]{1,0:T(8,128)(2,1)S(1)} %get-tuple-element.36), channel_id=1, source_target_pairs={{0,2},{1,3},{2,0},{3,1},{4,6},{5,7},{6,4},{7,5},{8,10},{9,11},{10,... | collective-permute-start | bytes 1179656 | tf_op jit(solution)/shard_map/ppermute | solution.py:346
  6.0 18.2 %collective-permute-start.7 = (bf16[32,4096]{1,0:T(8,128)(2,1)S(1)}, bf16[32,4096]{1,0:T(8,128)(2,1)S(1)}, u32[]{:S(2)}, u32[]{:S(2)}) collective-permute-start(bf16[32,4096]{1,0:T(8,128)(2,1)S(1)} %shard_map.82), channel_id=1, source_target_pairs={{0,2},{1,3},{2,0},{3,1},{4,6},{5,7},{6,4},{7,5},{8,10},{9,11},{10,... | collective-permute-start | bytes 786440 | tf_op jit(solution)/shard_map/ppermute | solution.py:346
  6.1 16.1 %collective-permute-start = (bf16[48,768]{1,0:T(8,128)(2,1)S(1)}, bf16[48,768]{1,0:T(8,128)(2,1)S(1)}, u32[]{:S(2)}, u32[]{:S(2)}) collective-permute-start(bf16[48,768]{1,0:T(8,128)(2,1)S(1)} %get-tuple-element.23), channel_id=1, source_target_pairs={{0,2},{1,3},{2,0},{3,1},{4,6},{5,7},{6,4},{7,5},{8,10},{9,11},{10,... | collective-permute-start | bytes 221192 | tf_op jit(solution)/shard_map/ppermute | solution.py:346
  8.1 20.7 %collective-permute-start.5 = (bf16[48,2048]{1,0:T(8,128)(2,1)S(1)}, bf16[48,2048]{1,0:T(8,128)(2,1)S(1)}, u32[]{:S(2)}, u32[]{:S(2)}) collective-permute-start(bf16[48,2048]{1,0:T(8,128)(2,1)S(1)} %get-tuple-element.28), channel_id=1, source_target_pairs={{0,2},{1,3},{2,0},{3,1},{4,6},{5,7},{6,4},{7,5},{8,10},{9,11},{10,... | collective-permute-start | bytes 589832 | tf_op jit(solution)/shard_map/ppermute | solution.py:346
  15.0 20.4 %collective-permute-start.10 = (bf16[48,4096]{1,0:T(8,128)(2,1)S(1)}, bf16[48,4096]{1,0:T(8,128)(2,1)S(1)}, u32[]{:S(2)}, u32[]{:S(2)}) collective-permute-start(bf16[48,4096]{1,0:T(8,128)(2,1)S(1)} %collective-permute-done.8.refs_1_), channel_id=1, source_target_pairs={{0,1},{1,0},{2,3},{3,2},{4,5},{5,4},{6,7},{7,6},{8,9},{9,8},{10,11... | collective-permute-start | bytes 1179656 | tf_op jit(solution)/shard_map/ppermute | solution.py:364
  22.2 6.6 %collective-permute-start.2 = (bf16[48,1280]{1,0:T(8,128)(2,1)S(1)}, bf16[48,1280]{1,0:T(8,128)(2,1)S(1)}, u32[]{:S(2)}, u32[]{:S(2)}) collective-permute-start(bf16[48,1280]{1,0:T(8,128)(2,1)S(1)} %get-tuple-element.24), channel_id=1, source_target_pairs={{0,2},{1,3},{2,0},{3,1},{4,6},{5,7},{6,4},{7,5},{8,10},{9,11},{10,... | collective-permute-start | bytes 368648 | tf_op jit(solution)/shard_map/ppermute | solution.py:346
  24.2 11.2 %collective-permute-start.9 = (bf16[32,4096]{1,0:T(8,128)(2,1)S(1)}, bf16[32,4096]{1,0:T(8,128)(2,1)S(1)}, u32[]{:S(2)}, u32[]{:S(2)}) collective-permute-start(bf16[32,4096]{1,0:T(8,128)(2,1)S(1)} %collective-permute-done.7.refs_0_), channel_id=1, source_target_pairs={{0,1},{1,0},{2,3},{3,2},{4,5},{5,4},{6,7},{7,6},{8,9},{9,8},{10,11... | collective-permute-start | bytes 786440 | tf_op jit(solution)/shard_map/ppermute | solution.py:364
  28.8 10.2 %collective-permute-start.1 = (bf16[48,768]{1,0:T(8,128)(2,1)S(1)}, bf16[48,768]{1,0:T(8,128)(2,1)S(1)}, u32[]{:S(2)}, u32[]{:S(2)}) collective-permute-start(bf16[48,768]{1,0:T(8,128)(2,1)S(1)} %collective-permute-done.xa), channel_id=1, source_target_pairs={{0,1},{1,0},{2,3},{3,2},{4,5},{5,4},{6,7},{7,6},{8,9},{9,8},{10,11... | collective-permute-start | bytes 221192 | tf_op jit(solution)/shard_map/ppermute | solution.py:364
  28.8 9.7 %collective-permute-start.3 = (bf16[48,1280]{1,0:T(8,128)(2,1)S(1)}, bf16[48,1280]{1,0:T(8,128)(2,1)S(1)}, u32[]{:S(2)}, u32[]{:S(2)}) collective-permute-start(bf16[48,1280]{1,0:T(8,128)(2,1)S(1)} %collective-permute-done.2.xa), channel_id=1, source_target_pairs={{0,1},{1,0},{2,3},{3,2},{4,5},{5,4},{6,7},{7,6},{8,9},{9,8},{10,11... | collective-permute-start | bytes 368648 | tf_op jit(solution)/shard_map/ppermute | solution.py:364
  29.3 8.3 %collective-permute-start.6 = (bf16[48,2048]{1,0:T(8,128)(2,1)S(1)}, bf16[48,2048]{1,0:T(8,128)(2,1)S(1)}, u32[]{:S(2)}, u32[]{:S(2)}) collective-permute-start(bf16[48,2048]{1,0:T(8,128)(2,1)S(1)} %collective-permute-done.5.xa), channel_id=1, source_target_pairs={{0,1},{1,0},{2,3},{3,2},{4,5},{5,4},{6,7},{7,6},{8,9},{9,8},{10,11... | collective-permute-start | bytes 589832 | tf_op jit(solution)/shard_map/ppermute | solution.py:364
  39.0 4.5 %copy-start.2 = (bf16[4,64]{1,0:T(4,128)(2,1)S(1)}, bf16[4,64]{1,0:T(4,128)(2,1)}, u32[]{:S(2)}) copy-start(bf16[4,64]{1,0:T(4,128)(2,1)} %question.1) | copy-start | bytes 1540
  39.9 4.6 %collective-permute-start.11 = (bf16[136,256]{1,0:T(8,128)(2,1)S(1)}, bf16[136,256]{1,0:T(8,128)(2,1)S(1)}, u32[]{:S(2)}, u32[]{:S(2)}) collective-permute-start(bf16[136,256]{1,0:T(8,128)(2,1)S(1)} %shard_map.84.refs_0_), channel_id=1, source_target_pairs={{0,4},{4,0},{8,12},{12,8},{16,20},{20,16},{24,28},{28,24},{1,5},{5... | collective-permute-start | bytes 208904 | tf_op jit(solution)/shard_map/ppermute | solution.py:410
  41.7 4.6 %collective-permute-start.12 = (bf16[136,256]{1,0:T(8,128)(2,1)S(1)}, bf16[136,256]{1,0:T(8,128)(2,1)S(1)}, u32[]{:S(2)}, u32[]{:S(2)}) collective-permute-start(bf16[136,256]{1,0:T(8,128)(2,1)S(1)} %shard_map.84.refs_0_), channel_id=1, source_target_pairs={{0,8},{4,12},{8,0},{12,4},{16,24},{20,28},{24,16},{28,20},{1,9},{5... | collective-permute-start | bytes 208904 | tf_op jit(solution)/shard_map/ppermute | solution.py:410
  43.3 5.2 %collective-permute-start.13 = (bf16[136,256]{1,0:T(8,128)(2,1)S(1)}, bf16[136,256]{1,0:T(8,128)(2,1)S(1)}, u32[]{:S(2)}, u32[]{:S(2)}) collective-permute-start(bf16[136,256]{1,0:T(8,128)(2,1)S(1)} %shard_map.84.refs_0_), channel_id=1, source_target_pairs={{0,12},{4,8},{8,4},{12,0},{16,28},{20,24},{24,20},{28,16},{1,13},{... | collective-permute-start | bytes 208904 | tf_op jit(solution)/shard_map/ppermute | solution.py:410
  48.8 6.1 %collective-permute-start.14 = (bf16[144,256]{1,0:T(8,128)(2,1)S(1)}, bf16[144,256]{1,0:T(8,128)(2,1)S(1)}, u32[]{:S(2)}, u32[]{:S(2)}) collective-permute-start(bf16[144,256]{1,0:T(8,128)(2,1)S(1)} %get-tuple-element.42.mine), channel_id=1, source_target_pairs={{0,16},{4,20},{8,24},{12,28},{16,0},{20,4},{24,8},{28,12},{1,17},{... | collective-permute-start | bytes 221192 | tf_op jit(solution)/shard_map/ppermute | solution.py:416

commit v3 on v2

--- a/solution.py
+++ b/solution.py
@@ -13,14 +13,13 @@
 DV = 128
 DECAY_TAU = 16.0
 ROW_PARTS = (2, 3, 3)
-COL_PARTS = (8, 5, 3)
+COL_PARTS = (16, 10, 3, 3)
 LATE = len(COL_PARTS)
 VMEM_LIMIT = 8 * 1024 * 1024
 
 
 F32 = jnp.float32
 BF16 = jnp.bfloat16
-EXACT = lax.Precision.HIGHEST
 
 
 def swap(count, bit):
@@ -136,9 +135,13 @@
 
 
 def against(left, state):
-    return lax.dot_general(
-        left, state, (((1,), (1,)), ((), ())), precision=EXACT, preferred_element_type=F32
-    )
+    left = left.astype(BF16)
+    dims = (((1,), (1,)), ((), ()))
+    high, mid, low = [
+        lax.dot_general(left, p.astype(BF16), dims, preferred_element_type=F32)
+        for p in split(state)
+    ]
+    return high + (mid + low)
 
 
 def cut_kernel(tokens, *refs, cuts):
@@ -361,7 +364,11 @@
     blocks, states, totals = [None], [s_near], [l_near]
     pairs = {}
     for bit, part in far:
-        pairs[bit, part] = (far[bit, part], lax.ppermute(far[bit, part], "tp", swap(tp, 1)))
+        if part == len(pieces) - 1:
+            other = lax.ppermute(pieces[part], "tp", swap(tp, 2 * bit + 1))
+        else:
+            other = lax.ppermute(far[bit, part], "tp", swap(tp, 1))
+        pairs[bit, part] = (far[bit, part], other)
     final_bit = tp // 2 - 1
     last = [pairs[final_bit, len(cuts) - LATE + n] for n in range(LATE)]
     for bit in range(1, tp // 2):

time: 56.1 us -> 55.9 us (level)
  waiting for transfers between devices: 27 us -> 22.9 us
  starting transfers between devices: 14.2 us -> 18 us
    ppermute x5 -> x6, waiting for transfers between devices: 18.6 us -> 14.7 us  [whole(): far[bit, part] = lax.ppermute(piece, 'tp', swap(tp, 2 * bit))]
    ppermute x5 -> x6, starting transfers between devices: 6.84 us -> 8.87 us  [whole(): far[bit, part] = lax.ppermute(piece, 'tp', swap(tp, 2 * bit))]
    ppermute x5 -> x6, starting transfers between devices: 0.59 us -> 2.34 us  [the longest x1 1.82 us: whole(): other = lax.ppermute(pieces[part], 'tp', swap(tp, 2 * bit + 1))]
    pallas_call x2 -> x3, Pallas kernels: 1.37 us -> 1.66 us  [whole(): call(functools.partial(partial_kernel, start=sides[n]), tuple((sds((late_...]
  transfers between devices with their start and end apart: 15 -> 17, of which waited for: 7 -> 7; matrix products, arithmetic and copies ran while one was open for 0% -> 0% of each run, Pallas kernels for 21% -> 22%
where the time goes in v3:
time: 55.9 us; the launch traced here: 55.7 us
  waiting for transfers between devices  22.9 us (41%)
  starting transfers between devices  18 us (32%)
  Pallas kernels  14.1 us (25%)
  between operations  0.79 us (1%)
    ppermute x6, waiting for transfers between devices, whole(): far[bit, part] = lax.ppermute(piece, 'tp', swap(tp, 2 * bit))  14.7 us
    ppermute x6, starting transfers between devices, whole(): far[bit, part] = lax.ppermute(piece, 'tp', swap(tp, 2 * bit))  8.87 us
    pallas_call x1, Pallas kernels, whole(): call(functools.partial(near_kernel, log_length=log_length), tuple((pltpu....  6.04 us
    ppermute x3, waiting for transfers between devices, whole(): others.append(lax.ppermute(payload, 'sp', swap(sp, far_bits)))  4.71 us
    ppermute x3, starting transfers between devices, whole(): others.append(lax.ppermute(payload, 'sp', swap(sp, far_bits)))  3.55 us
    ppermute x1, waiting for transfers between devices, whole(): other = lax.ppermute(payload, 'sp', swap(sp, bits[0]))  3.45 us
    ppermute x1, starting transfers between devices, whole(): other = lax.ppermute(payload, 'sp', swap(sp, bits[0]))  2.66 us
    pallas_call x1, Pallas kernels, whole(): call(functools.partial(early_kernel, log_length=log_length, pieces=len(ta...  2.19 us
  transfers between devices with their start and end apart: 17, of which 7 were waited for; matrix products, arithmetic and copies ran while one was open for 0% of the time, Pallas kernels for 22%

profile of v3, /device:TPU:0, one launch (start us, length us, event | category | flops | bytes accessed | tf_op | source)
XLA Modules:
  0.0 55.7 jit_solution(8365164042809338175)
XLA Ops:
  0.7 0.6 %collective-permute-start.4 = (bf16[128,4096]{1,0:T(8,128)(2,1)}, bf16[128,4096]{1,0:T(8,128)(2,1)S(1)}, u32[]{:S(2)}, u32[]{:S(2)}) collective-permute-start(bf16[128,4096]{1,0:T(8,128)(2,1)} %tokens.3), channel_id=1, source_target_pairs={{0,1},{1,0},{2,3},{3,2},{4,5},{5,4},{6,7},{7,6},{8,9},{9,8},{10,11... | collective-permute-start | bytes 3145736 | tf_op jit(solution)/shard_map/ppermute | solution.py:350
  1.2 1.2 %shard_map.78 = (bf16[48,4096]{1,0:T(8,128)(2,1)S(1)}, bf16[48,2048]{1,0:T(8,128)(2,1)S(1)}, bf16[48,1280]{1,0:T(8,128)(2,1)S(1)}, bf16[48,384]{1,0:T(8,128)(2,1)S(1)}, bf16[48,384]{1,0:T(8,128)(2,1)S(1)}) custom-call(bf16[128,4096]{1,0:T(8,128)(2,1)} %tokens.3), custom_call_target="tpu_custom_call" | custom-call | tf_op jit(solution)/shard_map/pallas_call | solution.py:340
  2.4 2.7 %collective-permute-start.10 = (bf16[48,4096]{1,0:T(8,128)(2,1)S(1)}, bf16[48,4096]{1,0:T(8,128)(2,1)S(1)}, u32[]{:S(2)}, u32[]{:S(2)}) collective-permute-start(bf16[48,4096]{1,0:T(8,128)(2,1)S(1)} %get-tuple-element.44), channel_id=1, source_target_pairs={{0,2},{1,3},{2,0},{3,1},{4,6},{5,7},{6,4},{7,5},{8,10},{9,11},{10,... | collective-permute-start | bytes 1179656 | tf_op jit(solution)/shard_map/ppermute | solution.py:349
  5.0 1.0 %shard_map.83 = bf16[32,4096]{1,0:T(8,128)(2,1)S(1)} custom-call(bf16[128,4096]{1,0:T(8,128)(2,1)} %tokens.3), custom_call_target="tpu_custom_call" | custom-call | tf_op jit(solution)/shard_map/pallas_call | solution.py:340
  6.0 0.1 collective-permute-start.9
  6.1 2.0 %collective-permute-start.7 = (bf16[48,2048]{1,0:T(8,128)(2,1)S(1)}, bf16[48,2048]{1,0:T(8,128)(2,1)S(1)}, u32[]{:S(2)}, u32[]{:S(2)}) collective-permute-start(bf16[48,2048]{1,0:T(8,128)(2,1)S(1)} %get-tuple-element.33), channel_id=1, source_target_pairs={{0,2},{1,3},{2,0},{3,1},{4,6},{5,7},{6,4},{7,5},{8,10},{9,11},{10,... | collective-permute-start | bytes 589832 | tf_op jit(solution)/shard_map/ppermute | solution.py:349
  8.1 6.9 %collective-permute-done.10.refs_1_ = bf16[48,4096]{1,0:T(8,128)(2,1)S(1)} collective-permute-done((bf16[48,4096]{1,0:T(8,128)(2,1)S(1)}, bf16[48,4096]{1,0:T(8,128)(2,1)S(1)}, u32[]{:S(2)}, u32[]{:S(2)}) %collective-permute-start.10) | collective-permute-done | bytes 393248 | tf_op jit(solution)/shard_map/ppermute | solution.py:349
  15.0 5.6 %collective-permute-done.9.refs_0_ = bf16[32,4096]{1,0:T(8,128)(2,1)S(1)} collective-permute-done((bf16[32,4096]{1,0:T(8,128)(2,1)S(1)}, bf16[32,4096]{1,0:T(8,128)(2,1)S(1)}, u32[]{:S(2)}, u32[]{:S(2)}) %collective-permute-start.9) | collective-permute-done | bytes 262176 | tf_op jit(solution)/shard_map/ppermute | solution.py:349
  20.6 2.0 %collective-permute-start.5 = (bf16[48,1280]{1,0:T(8,128)(2,1)S(1)}, bf16[48,1280]{1,0:T(8,128)(2,1)S(1)}, u32[]{:S(2)}, u32[]{:S(2)}) collective-permute-start(bf16[48,1280]{1,0:T(8,128)(2,1)S(1)} %get-tuple-element.32), channel_id=1, source_target_pairs={{0,2},{1,3},{2,0},{3,1},{4,6},{5,7},{6,4},{7,5},{8,10},{9,11},{10,... | collective-permute-start | bytes 368648 | tf_op jit(solution)/shard_map/ppermute | solution.py:349
  22.6 2.2 %collective-permute-done.7.xa = bf16[48,2048]{1,0:T(8,128)(2,1)S(1)} collective-permute-done((bf16[48,2048]{1,0:T(8,128)(2,1)S(1)}, bf16[48,2048]{1,0:T(8,128)(2,1)S(1)}, u32[]{:S(2)}, u32[]{:S(2)}) %collective-permute-start.7) | collective-permute-done | bytes 196640 | tf_op jit(solution)/shard_map/ppermute | solution.py:349
  24.8 2.0 %collective-permute-start.2 = (bf16[48,384]{1,0:T(8,128)(2,1)S(1)}, bf16[48,384]{1,0:T(8,128)(2,1)S(1)}, u32[]{:S(2)}, u32[]{:S(2)}) collective-permute-start(bf16[48,384]{1,0:T(8,128)(2,1)S(1)} %get-tuple-element.28), channel_id=1, source_target_pairs={{0,2},{1,3},{2,0},{3,1},{4,6},{5,7},{6,4},{7,5},{8,10},{9,11},{10,... | collective-permute-start | bytes 110600 | tf_op jit(solution)/shard_map/ppermute | solution.py:349
  26.9 6.0 %shard_map.79 = (bf16[4096,256]{1,0:T(8,128)(2,1)S(1)}, bf16[4096,512]{1,0:T(8,128)(2,1)S(1)}, bf16[4096,256]{1,0:T(8,128)(2,1)S(1)}, f32[128,256]{1,0:T(8,128)S(1)}, f32[1,256]{1,0:T(1,128)S(1)}) custom-call(bf16[128,4096]{1,0:T(8,128)(2,1)S(1)} %copy-done, bf16[128,4096]{1,0:T(8,128)(2,1)S(1)} %collective-permute-done.4.x1, bf16[4096,256]{1,0:T(8,128)(2,1)} %refs_0_.1, ...), custom_call_target="tpu_custom_call" | custom-call | flops 2147483648 | tf_op jit(solution)/shard_map/pallas_call | solution.py:354
  32.9 0.1 collective-permute-start
  33.0 1.8 %collective-permute-start.1 = (bf16[48,384]{1,0:T(8,128)(2,1)S(1)}, bf16[48,384]{1,0:T(8,128)(2,1)S(1)}, u32[]{:S(2)}, u32[]{:S(2)}) collective-permute-start(bf16[48,384]{1,0:T(8,128)(2,1)S(1)} %get-tuple-element.27), channel_id=1, source_target_pairs={{0,3},{1,2},{2,1},{3,0},{4,7},{5,6},{6,5},{7,4},{8,11},{9,10},{10,... | collective-permute-start | bytes 110600 | tf_op jit(solution)/shard_map/ppermute | solution.py:368
  34.8 0.3 collective-permute-start.3
  35.1 0.2 collective-permute-start.6
  35.4 2.2 %shard_map.84 = (f32[128,256]{1,0:T(8,128)S(1)}, f32[128,256]{1,0:T(8,128)S(1)}, f32[1,256]{1,0:T(1,128)S(1)}, f32[1,256]{1,0:T(1,128)S(1)}) custom-call(bf16[32,4096]{1,0:T(8,128)(2,1)S(1)} %collective-permute-done.9.refs_0_, bf16[48,4096]{1,0:T(8,128)(2,1)S(1)} %collective-permute-done.10.refs_1_, bf16[32,4096]{1,0:T(8,128)(2,1)S(1)} %collective-permute-done.11.refs_2_, ...), custom_call_target="tpu_custom_call" | custom-call | flops 1342177280 | tf_op jit(solution)/shard_map/pallas_call | solution.py:378
  37.6 0.8 %shard_map.80 = (f32[96,256]{1,0:T(8,128)S(1)}, f32[96,512]{1,0:T(8,128)S(1)}, f32[96,256]{1,0:T(8,128)S(1)}) custom-call(bf16[48,2048]{1,0:T(8,128)(2,1)S(1)} %collective-permute-done.7.xa, bf16[48,2048]{1,0:T(8,128)(2,1)S(1)} %collective-permute-done.8.xb, bf16[4096,256]{1,0:T(8,128)(2,1)S(1)} %get-tuple-element.29.wk.refs_4_, ...), custom_call_target="tpu_custom_call" | custom-call | flops 402653184 | tf_op jit(solution)/shard_map/pallas_call | solution.py:395
  38.4 0.6 %shard_map.81 = (f32[96,256]{1,0:T(8,128)S(1)}, f32[96,512]{1,0:T(8,128)S(1)}, f32[96,256]{1,0:T(8,128)S(1)}) custom-call(bf16[48,1280]{1,0:T(8,128)(2,1)S(1)} %collective-permute-done.5.xa, bf16[48,1280]{1,0:T(8,128)(2,1)S(1)} %collective-permute-done.6.xb, bf16[4096,256]{1,0:T(8,128)(2,1)S(1)} %get-tuple-element.29.wk.refs_4_, ...), custom_call_target="tpu_custom_call" | custom-call | flops 251658240 | tf_op jit(solution)/shard_map/pallas_call | solution.py:395
  39.0 0.3 shard_map.82
  39.3 0.8 %shard_map.85.refs_0_ = bf16[136,256]{1,0:T(8,128)(2,1)S(1)} custom-call(bf16[48,384]{1,0:T(8,128)(2,1)S(1)} %collective-permute-done.xa, bf16[48,384]{1,0:T(8,128)(2,1)S(1)} %collective-permute-done.1.xb, f32[96,256]{1,0:T(8,128)S(1)} %get-tuple-element.40.ks, f32[96,512]{1,0:T(8,128)S(1)} %get-tuple-element.41.vs, f32[96,256]{1,0:T(8,128)S(1)} %get-tuple-element.42.ds, ...), custom_call_target="tpu_custom_call" | custom-call | flops 75497472 | tf_op jit(solution)/shard_map/pallas_call | solution.py:401
  40.1 1.6 %collective-permute-start.13 = (bf16[136,256]{1,0:T(8,128)(2,1)S(1)}, bf16[136,256]{1,0:T(8,128)(2,1)S(1)}, u32[]{:S(2)}, u32[]{:S(2)}) collective-permute-start(bf16[136,256]{1,0:T(8,128)(2,1)S(1)} %shard_map.85.refs_0_), channel_id=1, source_target_pairs={{0,4},{4,0},{8,12},{12,8},{16,20},{20,16},{24,28},{28,24},{1,5},{5... | collective-permute-start | bytes 208904 | tf_op jit(solution)/shard_map/ppermute | solution.py:417
  41.6 1.6 %collective-permute-start.14 = (bf16[136,256]{1,0:T(8,128)(2,1)S(1)}, bf16[136,256]{1,0:T(8,128)(2,1)S(1)}, u32[]{:S(2)}, u32[]{:S(2)}) collective-permute-start(bf16[136,256]{1,0:T(8,128)(2,1)S(1)} %shard_map.85.refs_0_), channel_id=1, source_target_pairs={{0,8},{4,12},{8,0},{12,4},{16,24},{20,28},{24,16},{28,20},{1,9},{5... | collective-permute-start | bytes 208904 | tf_op jit(solution)/shard_map/ppermute | solution.py:417
  43.2 0.4 collective-permute-start.15
  43.6 0.1 shard_map.77.asked
  43.7 0.8 %collective-permute-done.13.refs_1_ = bf16[136,256]{1,0:T(8,128)(2,1)S(1)} collective-permute-done((bf16[136,256]{1,0:T(8,128)(2,1)S(1)}, bf16[136,256]{1,0:T(8,128)(2,1)S(1)}, u32[]{:S(2)}, u32[]{:S(2)}) %collective-permute-start.13) | collective-permute-done | bytes 69664 | tf_op jit(solution)/shard_map/ppermute | solution.py:417
  44.5 1.8 %collective-permute-done.14.refs_2_ = bf16[136,256]{1,0:T(8,128)(2,1)S(1)} collective-permute-done((bf16[136,256]{1,0:T(8,128)(2,1)S(1)}, bf16[136,256]{1,0:T(8,128)(2,1)S(1)}, u32[]{:S(2)}, u32[]{:S(2)}) %collective-permute-start.14) | collective-permute-done | bytes 69664 | tf_op jit(solution)/shard_map/ppermute | solution.py:417
  46.4 2.1 %collective-permute-done.15.refs_3_ = bf16[136,256]{1,0:T(8,128)(2,1)S(1)} collective-permute-done((bf16[136,256]{1,0:T(8,128)(2,1)S(1)}, bf16[136,256]{1,0:T(8,128)(2,1)S(1)}, u32[]{:S(2)}, u32[]{:S(2)}) %collective-permute-start.15) | collective-permute-done | bytes 69664 | tf_op jit(solution)/shard_map/ppermute | solution.py:417
  48.4 0.3 shard_map.86
  48.7 2.7 %collective-permute-start.16 = (bf16[144,256]{1,0:T(8,128)(2,1)S(1)}, bf16[144,256]{1,0:T(8,128)(2,1)S(1)}, u32[]{:S(2)}, u32[]{:S(2)}) collective-permute-start(bf16[144,256]{1,0:T(8,128)(2,1)S(1)} %get-tuple-element.50.mine), channel_id=1, source_target_pairs={{0,16},{4,20},{8,24},{12,28},{16,0},{20,4},{24,8},{28,12},{1,17},{... | collective-permute-start | bytes 221192 | tf_op jit(solution)/shard_map/ppermute | solution.py:423
  51.4 3.5 %collective-permute-done.16.other = bf16[144,256]{1,0:T(8,128)(2,1)S(1)} collective-permute-done((bf16[144,256]{1,0:T(8,128)(2,1)S(1)}, bf16[144,256]{1,0:T(8,128)(2,1)S(1)}, u32[]{:S(2)}, u32[]{:S(2)}) %collective-permute-start.16) | collective-permute-done | bytes 73760 | tf_op jit(solution)/shard_map/ppermute | solution.py:423
  54.8 0.9 %shard_map.87 = (bf16[4,8,128]{2,1,0:T(8,128)(2,1)}, bf16[4,128]{1,0:T(4,128)(2,1)}) custom-call(f32[8,256]{1,0:T(8,128)S(1)} %shard_map.77.asked, bf16[144,256]{1,0:T(8,128)(2,1)S(1)} %get-tuple-element.50.mine, bf16[144,256]{1,0:T(8,128)(2,1)S(1)} %collective-permute-done.16.other, f32[128,256]{1,0:T(8,128)S(1)} %get-tuple-element.51.exact), custom_call_target="tpu_custom_call" | custom-call | tf_op jit(solution)/shard_map/pallas_call | solution.py:425
  (19 shorter events, 0.1 us)
Async XLA Ops:
  0.6 26.2 %copy-start = (bf16[128,4096]{1,0:T(8,128)(2,1)S(1)}, bf16[128,4096]{1,0:T(8,128)(2,1)}, u32[]{:S(2)}) copy-start(bf16[128,4096]{1,0:T(8,128)(2,1)} %tokens.3) | copy-start | bytes 3145732
  0.6 26.2 %copy-start.1 = (f32[256]{0:T(256)S(1)}, f32[256]{0:T(256)}, u32[]{:S(2)}) copy-start(f32[256]{0:T(256)} %param.10) | copy-start | bytes 3076
  0.7 26.2 %collective-permute-start.4 = (bf16[128,4096]{1,0:T(8,128)(2,1)}, bf16[128,4096]{1,0:T(8,128)(2,1)S(1)}, u32[]{:S(2)}, u32[]{:S(2)}) collective-permute-start(bf16[128,4096]{1,0:T(8,128)(2,1)} %tokens.3), channel_id=1, source_target_pairs={{0,1},{1,0},{2,3},{3,2},{4,5},{5,4},{6,7},{7,6},{8,9},{9,8},{10,11... | collective-permute-start | bytes 3145736 | tf_op jit(solution)/shard_map/ppermute | solution.py:350
  2.4 12.6 %collective-permute-start.10 = (bf16[48,4096]{1,0:T(8,128)(2,1)S(1)}, bf16[48,4096]{1,0:T(8,128)(2,1)S(1)}, u32[]{:S(2)}, u32[]{:S(2)}) collective-permute-start(bf16[48,4096]{1,0:T(8,128)(2,1)S(1)} %get-tuple-element.44), channel_id=1, source_target_pairs={{0,2},{1,3},{2,0},{3,1},{4,6},{5,7},{6,4},{7,5},{8,10},{9,11},{10,... | collective-permute-start | bytes 1179656 | tf_op jit(solution)/shard_map/ppermute | solution.py:349
  6.0 14.6 %collective-permute-start.9 = (bf16[32,4096]{1,0:T(8,128)(2,1)S(1)}, bf16[32,4096]{1,0:T(8,128)(2,1)S(1)}, u32[]{:S(2)}, u32[]{:S(2)}) collective-permute-start(bf16[32,4096]{1,0:T(8,128)(2,1)S(1)} %shard_map.83), channel_id=1, source_target_pairs={{0,2},{1,3},{2,0},{3,1},{4,6},{5,7},{6,4},{7,5},{8,10},{9,11},{10,... | collective-permute-start | bytes 786440 | tf_op jit(solution)/shard_map/ppermute | solution.py:349
  6.1 18.7 %collective-permute-start.7 = (bf16[48,2048]{1,0:T(8,128)(2,1)S(1)}, bf16[48,2048]{1,0:T(8,128)(2,1)S(1)}, u32[]{:S(2)}, u32[]{:S(2)}) collective-permute-start(bf16[48,2048]{1,0:T(8,128)(2,1)S(1)} %get-tuple-element.33), channel_id=1, source_target_pairs={{0,2},{1,3},{2,0},{3,1},{4,6},{5,7},{6,4},{7,5},{8,10},{9,11},{10,... | collective-permute-start | bytes 589832 | tf_op jit(solution)/shard_map/ppermute | solution.py:349
  15.0 20.1 %collective-permute-start.12 = (bf16[48,4096]{1,0:T(8,128)(2,1)S(1)}, bf16[48,4096]{1,0:T(8,128)(2,1)S(1)}, u32[]{:S(2)}, u32[]{:S(2)}) collective-permute-start(bf16[48,4096]{1,0:T(8,128)(2,1)S(1)} %collective-permute-done.10.refs_1_), channel_id=1, source_target_pairs={{0,1},{1,0},{2,3},{3,2},{4,5},{5,4},{6,7},{7,6},{8,9},{9,8},{10,11... | collective-permute-start | bytes 1179656 | tf_op jit(solution)/shard_map/ppermute | solution.py:370
  20.6 14.2 %collective-permute-start.11 = (bf16[32,4096]{1,0:T(8,128)(2,1)S(1)}, bf16[32,4096]{1,0:T(8,128)(2,1)S(1)}, u32[]{:S(2)}, u32[]{:S(2)}) collective-permute-start(bf16[32,4096]{1,0:T(8,128)(2,1)S(1)} %collective-permute-done.9.refs_0_), channel_id=1, source_target_pairs={{0,1},{1,0},{2,3},{3,2},{4,5},{5,4},{6,7},{7,6},{8,9},{9,8},{10,11... | collective-permute-start | bytes 786440 | tf_op jit(solution)/shard_map/ppermute | solution.py:370
  20.6 12.4 %collective-permute-start.5 = (bf16[48,1280]{1,0:T(8,128)(2,1)S(1)}, bf16[48,1280]{1,0:T(8,128)(2,1)S(1)}, u32[]{:S(2)}, u32[]{:S(2)}) collective-permute-start(bf16[48,1280]{1,0:T(8,128)(2,1)S(1)} %get-tuple-element.32), channel_id=1, source_target_pairs={{0,2},{1,3},{2,0},{3,1},{4,6},{5,7},{6,4},{7,5},{8,10},{9,11},{10,... | collective-permute-start | bytes 368648 | tf_op jit(solution)/shard_map/ppermute | solution.py:349
  24.8 8.1 %collective-permute-start.2 = (bf16[48,384]{1,0:T(8,128)(2,1)S(1)}, bf16[48,384]{1,0:T(8,128)(2,1)S(1)}, u32[]{:S(2)}, u32[]{:S(2)}) collective-permute-start(bf16[48,384]{1,0:T(8,128)(2,1)S(1)} %get-tuple-element.28), channel_id=1, source_target_pairs={{0,2},{1,3},{2,0},{3,1},{4,6},{5,7},{6,4},{7,5},{8,10},{9,11},{10,... | collective-permute-start | bytes 110600 | tf_op jit(solution)/shard_map/ppermute | solution.py:349
  26.9 10.7 %collective-permute-start.8 = (bf16[48,2048]{1,0:T(8,128)(2,1)S(1)}, bf16[48,2048]{1,0:T(8,128)(2,1)S(1)}, u32[]{:S(2)}, u32[]{:S(2)}) collective-permute-start(bf16[48,2048]{1,0:T(8,128)(2,1)S(1)} %collective-permute-done.7.xa), channel_id=1, source_target_pairs={{0,1},{1,0},{2,3},{3,2},{4,5},{5,4},{6,7},{7,6},{8,9},{9,8},{10,11... | collective-permute-start | bytes 589832 | tf_op jit(solution)/shard_map/ppermute | solution.py:370
  32.9 6.3 %collective-permute-start = (bf16[48,384]{1,0:T(8,128)(2,1)S(1)}, bf16[48,384]{1,0:T(8,128)(2,1)S(1)}, u32[]{:S(2)}, u32[]{:S(2)}) collective-permute-start(bf16[48,384]{1,0:T(8,128)(2,1)S(1)} %get-tuple-element.27), channel_id=1, source_target_pairs={{0,2},{1,3},{2,0},{3,1},{4,6},{5,7},{6,4},{7,5},{8,10},{9,11},{10,... | collective-permute-start | bytes 110600 | tf_op jit(solution)/shard_map/ppermute | solution.py:349
  33.0 6.2 %collective-permute-start.1 = (bf16[48,384]{1,0:T(8,128)(2,1)S(1)}, bf16[48,384]{1,0:T(8,128)(2,1)S(1)}, u32[]{:S(2)}, u32[]{:S(2)}) collective-permute-start(bf16[48,384]{1,0:T(8,128)(2,1)S(1)} %get-tuple-element.27), channel_id=1, source_target_pairs={{0,3},{1,2},{2,1},{3,0},{4,7},{5,6},{6,5},{7,4},{8,11},{9,10},{10,... | collective-permute-start | bytes 110600 | tf_op jit(solution)/shard_map/ppermute | solution.py:368
  34.8 4.1 %collective-permute-start.3 = (bf16[48,384]{1,0:T(8,128)(2,1)S(1)}, bf16[48,384]{1,0:T(8,128)(2,1)S(1)}, u32[]{:S(2)}, u32[]{:S(2)}) collective-permute-start(bf16[48,384]{1,0:T(8,128)(2,1)S(1)} %collective-permute-done.2.xa), channel_id=1, source_target_pairs={{0,1},{1,0},{2,3},{3,2},{4,5},{5,4},{6,7},{7,6},{8,9},{9,8},{10,11... | collective-permute-start | bytes 110600 | tf_op jit(solution)/shard_map/ppermute | solution.py:370
  35.1 3.2 %collective-permute-start.6 = (bf16[48,1280]{1,0:T(8,128)(2,1)S(1)}, bf16[48,1280]{1,0:T(8,128)(2,1)S(1)}, u32[]{:S(2)}, u32[]{:S(2)}) collective-permute-start(bf16[48,1280]{1,0:T(8,128)(2,1)S(1)} %collective-permute-done.5.xa), channel_id=1, source_target_pairs={{0,1},{1,0},{2,3},{3,2},{4,5},{5,4},{6,7},{7,6},{8,9},{9,8},{10,11... | collective-permute-start | bytes 368648 | tf_op jit(solution)/shard_map/ppermute | solution.py:370
  39.3 4.4 %copy-start.2 = (bf16[4,64]{1,0:T(4,128)(2,1)S(1)}, bf16[4,64]{1,0:T(4,128)(2,1)}, u32[]{:S(2)}) copy-start(bf16[4,64]{1,0:T(4,128)(2,1)} %question.1) | copy-start | bytes 1540
  40.1 4.5 %collective-permute-start.13 = (bf16[136,256]{1,0:T(8,128)(2,1)S(1)}, bf16[136,256]{1,0:T(8,128)(2,1)S(1)}, u32[]{:S(2)}, u32[]{:S(2)}) collective-permute-start(bf16[136,256]{1,0:T(8,128)(2,1)S(1)} %shard_map.85.refs_0_), channel_id=1, source_target_pairs={{0,4},{4,0},{8,12},{12,8},{16,20},{20,16},{24,28},{28,24},{1,5},{5... | collective-permute-start | bytes 208904 | tf_op jit(solution)/shard_map/ppermute | solution.py:417
  41.6 4.7 %collective-permute-start.14 = (bf16[136,256]{1,0:T(8,128)(2,1)S(1)}, bf16[136,256]{1,0:T(8,128)(2,1)S(1)}, u32[]{:S(2)}, u32[]{:S(2)}) collective-permute-start(bf16[136,256]{1,0:T(8,128)(2,1)S(1)} %shard_map.85.refs_0_), channel_id=1, source_target_pairs={{0,8},{4,12},{8,0},{12,4},{16,24},{20,28},{24,16},{28,20},{1,9},{5... | collective-permute-start | bytes 208904 | tf_op jit(solution)/shard_map/ppermute | solution.py:417
  43.2 5.2 %collective-permute-start.15 = (bf16[136,256]{1,0:T(8,128)(2,1)S(1)}, bf16[136,256]{1,0:T(8,128)(2,1)S(1)}, u32[]{:S(2)}, u32[]{:S(2)}) collective-permute-start(bf16[136,256]{1,0:T(8,128)(2,1)S(1)} %shard_map.85.refs_0_), channel_id=1, source_target_pairs={{0,12},{4,8},{8,4},{12,0},{16,28},{20,24},{24,20},{28,16},{1,13},{... | collective-permute-start | bytes 208904 | tf_op jit(solution)/shard_map/ppermute | solution.py:417
  48.7 6.1 %collective-permute-start.16 = (bf16[144,256]{1,0:T(8,128)(2,1)S(1)}, bf16[144,256]{1,0:T(8,128)(2,1)S(1)}, u32[]{:S(2)}, u32[]{:S(2)}) collective-permute-start(bf16[144,256]{1,0:T(8,128)(2,1)S(1)} %get-tuple-element.50.mine), channel_id=1, source_target_pairs={{0,16},{4,20},{8,24},{12,28},{16,0},{20,4},{24,8},{28,12},{1,17},{... | collective-permute-start | bytes 221192 | tf_op jit(solution)/shard_map/ppermute | solution.py:423

commit v4 on v3

--- a/solution.py
+++ b/solution.py
@@ -13,7 +13,7 @@
 DV = 128
 DECAY_TAU = 16.0
 ROW_PARTS = (2, 3, 3)
-COL_PARTS = (16, 10, 3, 3)
+COL_PARTS = (8, 5, 3)
 LATE = len(COL_PARTS)
 VMEM_LIMIT = 8 * 1024 * 1024
 
@@ -364,11 +364,7 @@
     blocks, states, totals = [None], [s_near], [l_near]
     pairs = {}
     for bit, part in far:
-        if part == len(pieces) - 1:
-            other = lax.ppermute(pieces[part], "tp", swap(tp, 2 * bit + 1))
-        else:
-            other = lax.ppermute(far[bit, part], "tp", swap(tp, 1))
-        pairs[bit, part] = (far[bit, part], other)
+        pairs[bit, part] = (far[bit, part], lax.ppermute(far[bit, part], "tp", swap(tp, 1)))
     final_bit = tp // 2 - 1
     last = [pairs[final_bit, len(cuts) - LATE + n] for n in range(LATE)]
     for bit in range(1, tp // 2):

time: 55.9 us -> 56 us (level)
  waiting for transfers between devices: 22.9 us -> 27 us
  starting transfers between devices: 18 us -> 14.2 us
    ppermute x6 -> x5, waiting for transfers between devices: 14.7 us -> 18.6 us  [whole(): far[bit, part] = lax.ppermute(piece, 'tp', swap(tp, 2 * bit))]
    ppermute x6 -> x5, starting transfers between devices: 8.87 us -> 6.84 us  [whole(): far[bit, part] = lax.ppermute(piece, 'tp', swap(tp, 2 * bit))]
    ppermute x6 -> x5, starting transfers between devices: 2.34 us -> 0.59 us  [whole(): lax.ppermute(far[bit, part], 'tp', swap(tp, 1))]
    pallas_call x3 -> x2, Pallas kernels: 1.66 us -> 1.37 us  [whole(): call(functools.partial(partial_kernel, start=sides[n]), tuple((sds((late_...]
  transfers between devices with their start and end apart: 17 -> 15, of which waited for: 7 -> 7; matrix products, arithmetic and copies ran while one was open for 0% -> 0% of each run, Pallas kernels for 22% -> 21%
where the time goes in v4:
time: 56 us; the launch traced here: 55.8 us
  waiting for transfers between devices  27 us (48%)
  starting transfers between devices  14.2 us (25%)
  Pallas kernels  13.9 us (25%)
  between operations  0.76 us (1%)
    ppermute x5, waiting for transfers between devices, whole(): far[bit, part] = lax.ppermute(piece, 'tp', swap(tp, 2 * bit))  18.6 us
    ppermute x5, starting transfers between devices, whole(): far[bit, part] = lax.ppermute(piece, 'tp', swap(tp, 2 * bit))  6.84 us
    pallas_call x1, Pallas kernels, whole(): call(functools.partial(near_kernel, log_length=log_length), tuple((pltpu....  6.03 us
    ppermute x3, waiting for transfers between devices, whole(): others.append(lax.ppermute(payload, 'sp', swap(sp, far_bits)))  4.94 us
    ppermute x3, starting transfers between devices, whole(): others.append(lax.ppermute(payload, 'sp', swap(sp, far_bits)))  3.55 us
    ppermute x1, waiting for transfers between devices, whole(): other = lax.ppermute(payload, 'sp', swap(sp, bits[0]))  3.45 us
    ppermute x1, starting transfers between devices, whole(): other = lax.ppermute(payload, 'sp', swap(sp, bits[0]))  2.64 us
    pallas_call x1, Pallas kernels, whole(): call(functools.partial(early_kernel, log_length=log_length, pieces=len(ta...  2.19 us
  transfers between devices with their start and end apart: 15, of which 7 were waited for; matrix products, arithmetic and copies ran while one was open for 0% of the time, Pallas kernels for 21%

profile of v4, /device:TPU:0, one launch (start us, length us, event | category | flops | bytes accessed | tf_op | source)
XLA Modules:
  0.0 55.8 jit_solution(10943603873000300147)
XLA Ops:
  0.6 0.0 copy-start
  0.7 0.6 collective-permute-start.4
  1.2 1.2 %shard_map.78 = (bf16[48,4096]{1,0:T(8,128)(2,1)S(1)}, bf16[48,2048]{1,0:T(8,128)(2,1)S(1)}, bf16[48,1280]{1,0:T(8,128)(2,1)S(1)}, bf16[48,768]{1,0:T(8,128)(2,1)S(1)}) custom-call(bf16[128,4096]{1,0:T(8,128)(2,1)} %tokens.3), custom_call_target="tpu_custom_call" | custom-call | tf_op jit(solution)/shard_map/pallas_call | solution.py:340
  2.4 2.7 %collective-permute-start.8 = (bf16[48,4096]{1,0:T(8,128)(2,1)S(1)}, bf16[48,4096]{1,0:T(8,128)(2,1)S(1)}, u32[]{:S(2)}, u32[]{:S(2)}) collective-permute-start(bf16[48,4096]{1,0:T(8,128)(2,1)S(1)} %get-tuple-element.36), channel_id=1, source_target_pairs={{0,2},{1,3},{2,0},{3,1},{4,6},{5,7},{6,4},{7,5},{8,10},{9,11},{10,... | collective-permute-start | bytes 1179656 | tf_op jit(solution)/shard_map/ppermute | solution.py:349
  5.0 1.0 %shard_map.82 = bf16[32,4096]{1,0:T(8,128)(2,1)S(1)} custom-call(bf16[128,4096]{1,0:T(8,128)(2,1)} %tokens.3), custom_call_target="tpu_custom_call" | custom-call | tf_op jit(solution)/shard_map/pallas_call | solution.py:340
  6.0 0.1 collective-permute-start.7
  6.1 2.0 %collective-permute-start = (bf16[48,768]{1,0:T(8,128)(2,1)S(1)}, bf16[48,768]{1,0:T(8,128)(2,1)S(1)}, u32[]{:S(2)}, u32[]{:S(2)}) collective-permute-start(bf16[48,768]{1,0:T(8,128)(2,1)S(1)} %get-tuple-element.23), channel_id=1, source_target_pairs={{0,2},{1,3},{2,0},{3,1},{4,6},{5,7},{6,4},{7,5},{8,10},{9,11},{10,... | collective-permute-start | bytes 221192 | tf_op jit(solution)/shard_map/ppermute | solution.py:349
  8.1 0.1 collective-permute-start.5
  8.2 6.8 %collective-permute-done.8.refs_1_ = bf16[48,4096]{1,0:T(8,128)(2,1)S(1)} collective-permute-done((bf16[48,4096]{1,0:T(8,128)(2,1)S(1)}, bf16[48,4096]{1,0:T(8,128)(2,1)S(1)}, u32[]{:S(2)}, u32[]{:S(2)}) %collective-permute-start.8) | collective-permute-done | bytes 393248 | tf_op jit(solution)/shard_map/ppermute | solution.py:349
  15.0 0.0 collective-permute-start.10
  15.0 7.2 %collective-permute-done.xa = bf16[48,768]{1,0:T(8,128)(2,1)S(1)} collective-permute-done((bf16[48,768]{1,0:T(8,128)(2,1)S(1)}, bf16[48,768]{1,0:T(8,128)(2,1)S(1)}, u32[]{:S(2)}, u32[]{:S(2)}) %collective-permute-start) | collective-permute-done | bytes 73760 | tf_op jit(solution)/shard_map/ppermute | solution.py:349
  22.2 2.0 %collective-permute-start.2 = (bf16[48,1280]{1,0:T(8,128)(2,1)S(1)}, bf16[48,1280]{1,0:T(8,128)(2,1)S(1)}, u32[]{:S(2)}, u32[]{:S(2)}) collective-permute-start(bf16[48,1280]{1,0:T(8,128)(2,1)S(1)} %get-tuple-element.24), channel_id=1, source_target_pairs={{0,2},{1,3},{2,0},{3,1},{4,6},{5,7},{6,4},{7,5},{8,10},{9,11},{10,... | collective-permute-start | bytes 368648 | tf_op jit(solution)/shard_map/ppermute | solution.py:349
  24.2 4.6 %collective-permute-done.2.xa = bf16[48,1280]{1,0:T(8,128)(2,1)S(1)} collective-permute-done((bf16[48,1280]{1,0:T(8,128)(2,1)S(1)}, bf16[48,1280]{1,0:T(8,128)(2,1)S(1)}, u32[]{:S(2)}, u32[]{:S(2)}) %collective-permute-start.2) | collective-permute-done | bytes 122912 | tf_op jit(solution)/shard_map/ppermute | solution.py:349
  28.8 0.5 collective-permute-start.3
  29.3 0.1 collective-permute-start.6
  29.4 6.0 %shard_map.79 = (bf16[4096,256]{1,0:T(8,128)(2,1)S(1)}, bf16[4096,512]{1,0:T(8,128)(2,1)S(1)}, bf16[4096,256]{1,0:T(8,128)(2,1)S(1)}, f32[128,256]{1,0:T(8,128)S(1)}, f32[1,256]{1,0:T(1,128)S(1)}) custom-call(bf16[128,4096]{1,0:T(8,128)(2,1)S(1)} %copy-done, bf16[128,4096]{1,0:T(8,128)(2,1)S(1)} %collective-permute-done.4.x1, bf16[4096,256]{1,0:T(8,128)(2,1)} %refs_0_.1, ...), custom_call_target="tpu_custom_call" | custom-call | flops 2147483648 | tf_op jit(solution)/shard_map/pallas_call | solution.py:354
  35.4 2.2 %shard_map.83 = (f32[128,256]{1,0:T(8,128)S(1)}, f32[128,256]{1,0:T(8,128)S(1)}, f32[1,256]{1,0:T(1,128)S(1)}, f32[1,256]{1,0:T(1,128)S(1)}) custom-call(bf16[32,4096]{1,0:T(8,128)(2,1)S(1)} %collective-permute-done.7.refs_0_, bf16[48,4096]{1,0:T(8,128)(2,1)S(1)} %collective-permute-done.8.refs_1_, bf16[32,4096]{1,0:T(8,128)(2,1)S(1)} %collective-permute-done.9.refs_2_, ...), custom_call_target="tpu_custom_call" | custom-call | flops 1342177280 | tf_op jit(solution)/shard_map/pallas_call | solution.py:374
  37.6 0.8 %shard_map.80 = (f32[96,256]{1,0:T(8,128)S(1)}, f32[96,512]{1,0:T(8,128)S(1)}, f32[96,256]{1,0:T(8,128)S(1)}) custom-call(bf16[48,2048]{1,0:T(8,128)(2,1)S(1)} %collective-permute-done.5.xa, bf16[48,2048]{1,0:T(8,128)(2,1)S(1)} %collective-permute-done.6.xb, bf16[4096,256]{1,0:T(8,128)(2,1)S(1)} %get-tuple-element.25.wk.refs_4_, ...), custom_call_target="tpu_custom_call" | custom-call | flops 402653184 | tf_op jit(solution)/shard_map/pallas_call | solution.py:391
  38.5 0.6 %shard_map.81 = (f32[96,256]{1,0:T(8,128)S(1)}, f32[96,512]{1,0:T(8,128)S(1)}, f32[96,256]{1,0:T(8,128)S(1)}) custom-call(bf16[48,1280]{1,0:T(8,128)(2,1)S(1)} %collective-permute-done.2.xa, bf16[48,1280]{1,0:T(8,128)(2,1)S(1)} %collective-permute-done.3.xb, bf16[4096,256]{1,0:T(8,128)(2,1)S(1)} %get-tuple-element.25.wk.refs_4_, ...), custom_call_target="tpu_custom_call" | custom-call | flops 251658240 | tf_op jit(solution)/shard_map/pallas_call | solution.py:391
  39.0 0.0 copy-start.2
  39.1 0.9 %shard_map.84.refs_0_ = bf16[136,256]{1,0:T(8,128)(2,1)S(1)} custom-call(bf16[48,768]{1,0:T(8,128)(2,1)S(1)} %collective-permute-done.xa, bf16[48,768]{1,0:T(8,128)(2,1)S(1)} %collective-permute-done.1.xb, f32[96,256]{1,0:T(8,128)S(1)} %get-tuple-element.32.ks, f32[96,512]{1,0:T(8,128)S(1)} %get-tuple-element.33.vs, f32[96,256]{1,0:T(8,128)S(1)} %get-tuple-element.34.ds, ...), custom_call_target="tpu_custom_call" | custom-call | flops 150994944 | tf_op jit(solution)/shard_map/pallas_call | solution.py:397
  39.9 1.8 %collective-permute-start.11 = (bf16[136,256]{1,0:T(8,128)(2,1)S(1)}, bf16[136,256]{1,0:T(8,128)(2,1)S(1)}, u32[]{:S(2)}, u32[]{:S(2)}) collective-permute-start(bf16[136,256]{1,0:T(8,128)(2,1)S(1)} %shard_map.84.refs_0_), channel_id=1, source_target_pairs={{0,4},{4,0},{8,12},{12,8},{16,20},{20,16},{24,28},{28,24},{1,5},{5... | collective-permute-start | bytes 208904 | tf_op jit(solution)/shard_map/ppermute | solution.py:413
  41.7 1.6 %collective-permute-start.12 = (bf16[136,256]{1,0:T(8,128)(2,1)S(1)}, bf16[136,256]{1,0:T(8,128)(2,1)S(1)}, u32[]{:S(2)}, u32[]{:S(2)}) collective-permute-start(bf16[136,256]{1,0:T(8,128)(2,1)S(1)} %shard_map.84.refs_0_), channel_id=1, source_target_pairs={{0,8},{4,12},{8,0},{12,4},{16,24},{20,28},{24,16},{28,20},{1,9},{5... | collective-permute-start | bytes 208904 | tf_op jit(solution)/shard_map/ppermute | solution.py:413
  43.3 0.2 collective-permute-start.13
  43.5 0.1 shard_map.77.asked
  43.6 1.0 %collective-permute-done.11.refs_1_ = bf16[136,256]{1,0:T(8,128)(2,1)S(1)} collective-permute-done((bf16[136,256]{1,0:T(8,128)(2,1)S(1)}, bf16[136,256]{1,0:T(8,128)(2,1)S(1)}, u32[]{:S(2)}, u32[]{:S(2)}) %collective-permute-start.11) | collective-permute-done | bytes 69664 | tf_op jit(solution)/shard_map/ppermute | solution.py:413
  44.5 1.8 %collective-permute-done.12.refs_2_ = bf16[136,256]{1,0:T(8,128)(2,1)S(1)} collective-permute-done((bf16[136,256]{1,0:T(8,128)(2,1)S(1)}, bf16[136,256]{1,0:T(8,128)(2,1)S(1)}, u32[]{:S(2)}, u32[]{:S(2)}) %collective-permute-start.12) | collective-permute-done | bytes 69664 | tf_op jit(solution)/shard_map/ppermute | solution.py:413
  46.3 2.2 %collective-permute-done.13.refs_3_ = bf16[136,256]{1,0:T(8,128)(2,1)S(1)} collective-permute-done((bf16[136,256]{1,0:T(8,128)(2,1)S(1)}, bf16[136,256]{1,0:T(8,128)(2,1)S(1)}, u32[]{:S(2)}, u32[]{:S(2)}) %collective-permute-start.13) | collective-permute-done | bytes 69664 | tf_op jit(solution)/shard_map/ppermute | solution.py:413
  48.5 0.3 shard_map.85
  48.8 2.6 %collective-permute-start.14 = (bf16[144,256]{1,0:T(8,128)(2,1)S(1)}, bf16[144,256]{1,0:T(8,128)(2,1)S(1)}, u32[]{:S(2)}, u32[]{:S(2)}) collective-permute-start(bf16[144,256]{1,0:T(8,128)(2,1)S(1)} %get-tuple-element.42.mine), channel_id=1, source_target_pairs={{0,16},{4,20},{8,24},{12,28},{16,0},{20,4},{24,8},{28,12},{1,17},{... | collective-permute-start | bytes 221192 | tf_op jit(solution)/shard_map/ppermute | solution.py:419
  51.5 3.5 %collective-permute-done.14.other = bf16[144,256]{1,0:T(8,128)(2,1)S(1)} collective-permute-done((bf16[144,256]{1,0:T(8,128)(2,1)S(1)}, bf16[144,256]{1,0:T(8,128)(2,1)S(1)}, u32[]{:S(2)}, u32[]{:S(2)}) %collective-permute-start.14) | collective-permute-done | bytes 73760 | tf_op jit(solution)/shard_map/ppermute | solution.py:419
  54.9 0.9 %shard_map.86 = (bf16[4,8,128]{2,1,0:T(8,128)(2,1)}, bf16[4,128]{1,0:T(4,128)(2,1)}) custom-call(f32[8,256]{1,0:T(8,128)S(1)} %shard_map.77.asked, bf16[144,256]{1,0:T(8,128)(2,1)S(1)} %get-tuple-element.42.mine, bf16[144,256]{1,0:T(8,128)(2,1)S(1)} %collective-permute-done.14.other, f32[128,256]{1,0:T(8,128)S(1)} %get-tuple-element.43.exact), custom_call_target="tpu_custom_call" | custom-call | tf_op jit(solution)/shard_map/pallas_call | solution.py:421
  (14 shorter events, 0.0 us)
Async XLA Ops:
  0.6 28.7 %copy-start = (bf16[128,4096]{1,0:T(8,128)(2,1)S(1)}, bf16[128,4096]{1,0:T(8,128)(2,1)}, u32[]{:S(2)}) copy-start(bf16[128,4096]{1,0:T(8,128)(2,1)} %tokens.3) | copy-start | bytes 3145732
  0.6 28.7 %copy-start.1 = (f32[256]{0:T(256)S(1)}, f32[256]{0:T(256)}, u32[]{:S(2)}) copy-start(f32[256]{0:T(256)} %param.10) | copy-start | bytes 3076
  0.7 28.7 %collective-permute-start.4 = (bf16[128,4096]{1,0:T(8,128)(2,1)}, bf16[128,4096]{1,0:T(8,128)(2,1)S(1)}, u32[]{:S(2)}, u32[]{:S(2)}) collective-permute-start(bf16[128,4096]{1,0:T(8,128)(2,1)} %tokens.3), channel_id=1, source_target_pairs={{0,1},{1,0},{2,3},{3,2},{4,5},{5,4},{6,7},{7,6},{8,9},{9,8},{10,11... | collective-permute-start | bytes 3145736 | tf_op jit(solution)/shard_map/ppermute | solution.py:350
  2.4 12.6 %collective-permute-start.8 = (bf16[48,4096]{1,0:T(8,128)(2,1)S(1)}, bf16[48,4096]{1,0:T(8,128)(2,1)S(1)}, u32[]{:S(2)}, u32[]{:S(2)}) collective-permute-start(bf16[48,4096]{1,0:T(8,128)(2,1)S(1)} %get-tuple-element.36), channel_id=1, source_target_pairs={{0,2},{1,3},{2,0},{3,1},{4,6},{5,7},{6,4},{7,5},{8,10},{9,11},{10,... | collective-permute-start | bytes 1179656 | tf_op jit(solution)/shard_map/ppermute | solution.py:349
  6.0 18.2 %collective-permute-start.7 = (bf16[32,4096]{1,0:T(8,128)(2,1)S(1)}, bf16[32,4096]{1,0:T(8,128)(2,1)S(1)}, u32[]{:S(2)}, u32[]{:S(2)}) collective-permute-start(bf16[32,4096]{1,0:T(8,128)(2,1)S(1)} %shard_map.82), channel_id=1, source_target_pairs={{0,2},{1,3},{2,0},{3,1},{4,6},{5,7},{6,4},{7,5},{8,10},{9,11},{10,... | collective-permute-start | bytes 786440 | tf_op jit(solution)/shard_map/ppermute | solution.py:349
  6.1 16.1 %collective-permute-start = (bf16[48,768]{1,0:T(8,128)(2,1)S(1)}, bf16[48,768]{1,0:T(8,128)(2,1)S(1)}, u32[]{:S(2)}, u32[]{:S(2)}) collective-permute-start(bf16[48,768]{1,0:T(8,128)(2,1)S(1)} %get-tuple-element.23), channel_id=1, source_target_pairs={{0,2},{1,3},{2,0},{3,1},{4,6},{5,7},{6,4},{7,5},{8,10},{9,11},{10,... | collective-permute-start | bytes 221192 | tf_op jit(solution)/shard_map/ppermute | solution.py:349
  8.1 20.7 %collective-permute-start.5 = (bf16[48,2048]{1,0:T(8,128)(2,1)S(1)}, bf16[48,2048]{1,0:T(8,128)(2,1)S(1)}, u32[]{:S(2)}, u32[]{:S(2)}) collective-permute-start(bf16[48,2048]{1,0:T(8,128)(2,1)S(1)} %get-tuple-element.28), channel_id=1, source_target_pairs={{0,2},{1,3},{2,0},{3,1},{4,6},{5,7},{6,4},{7,5},{8,10},{9,11},{10,... | collective-permute-start | bytes 589832 | tf_op jit(solution)/shard_map/ppermute | solution.py:349
  15.0 20.4 %collective-permute-start.10 = (bf16[48,4096]{1,0:T(8,128)(2,1)S(1)}, bf16[48,4096]{1,0:T(8,128)(2,1)S(1)}, u32[]{:S(2)}, u32[]{:S(2)}) collective-permute-start(bf16[48,4096]{1,0:T(8,128)(2,1)S(1)} %collective-permute-done.8.refs_1_), channel_id=1, source_target_pairs={{0,1},{1,0},{2,3},{3,2},{4,5},{5,4},{6,7},{7,6},{8,9},{9,8},{10,11... | collective-permute-start | bytes 1179656 | tf_op jit(solution)/shard_map/ppermute | solution.py:367
  22.2 6.6 %collective-permute-start.2 = (bf16[48,1280]{1,0:T(8,128)(2,1)S(1)}, bf16[48,1280]{1,0:T(8,128)(2,1)S(1)}, u32[]{:S(2)}, u32[]{:S(2)}) collective-permute-start(bf16[48,1280]{1,0:T(8,128)(2,1)S(1)} %get-tuple-element.24), channel_id=1, source_target_pairs={{0,2},{1,3},{2,0},{3,1},{4,6},{5,7},{6,4},{7,5},{8,10},{9,11},{10,... | collective-permute-start | bytes 368648 | tf_op jit(solution)/shard_map/ppermute | solution.py:349
  24.2 11.2 %collective-permute-start.9 = (bf16[32,4096]{1,0:T(8,128)(2,1)S(1)}, bf16[32,4096]{1,0:T(8,128)(2,1)S(1)}, u32[]{:S(2)}, u32[]{:S(2)}) collective-permute-start(bf16[32,4096]{1,0:T(8,128)(2,1)S(1)} %collective-permute-done.7.refs_0_), channel_id=1, source_target_pairs={{0,1},{1,0},{2,3},{3,2},{4,5},{5,4},{6,7},{7,6},{8,9},{9,8},{10,11... | collective-permute-start | bytes 786440 | tf_op jit(solution)/shard_map/ppermute | solution.py:367
  28.8 10.2 %collective-permute-start.1 = (bf16[48,768]{1,0:T(8,128)(2,1)S(1)}, bf16[48,768]{1,0:T(8,128)(2,1)S(1)}, u32[]{:S(2)}, u32[]{:S(2)}) collective-permute-start(bf16[48,768]{1,0:T(8,128)(2,1)S(1)} %collective-permute-done.xa), channel_id=1, source_target_pairs={{0,1},{1,0},{2,3},{3,2},{4,5},{5,4},{6,7},{7,6},{8,9},{9,8},{10,11... | collective-permute-start | bytes 221192 | tf_op jit(solution)/shard_map/ppermute | solution.py:367
  28.8 9.7 %collective-permute-start.3 = (bf16[48,1280]{1,0:T(8,128)(2,1)S(1)}, bf16[48,1280]{1,0:T(8,128)(2,1)S(1)}, u32[]{:S(2)}, u32[]{:S(2)}) collective-permute-start(bf16[48,1280]{1,0:T(8,128)(2,1)S(1)} %collective-permute-done.2.xa), channel_id=1, source_target_pairs={{0,1},{1,0},{2,3},{3,2},{4,5},{5,4},{6,7},{7,6},{8,9},{9,8},{10,11... | collective-permute-start | bytes 368648 | tf_op jit(solution)/shard_map/ppermute | solution.py:367
  29.3 8.3 %collective-permute-start.6 = (bf16[48,2048]{1,0:T(8,128)(2,1)S(1)}, bf16[48,2048]{1,0:T(8,128)(2,1)S(1)}, u32[]{:S(2)}, u32[]{:S(2)}) collective-permute-start(bf16[48,2048]{1,0:T(8,128)(2,1)S(1)} %collective-permute-done.5.xa), channel_id=1, source_target_pairs={{0,1},{1,0},{2,3},{3,2},{4,5},{5,4},{6,7},{7,6},{8,9},{9,8},{10,11... | collective-permute-start | bytes 589832 | tf_op jit(solution)/shard_map/ppermute | solution.py:367
  39.0 4.5 %copy-start.2 = (bf16[4,64]{1,0:T(4,128)(2,1)S(1)}, bf16[4,64]{1,0:T(4,128)(2,1)}, u32[]{:S(2)}) copy-start(bf16[4,64]{1,0:T(4,128)(2,1)} %question.1) | copy-start | bytes 1540
  39.9 4.6 %collective-permute-start.11 = (bf16[136,256]{1,0:T(8,128)(2,1)S(1)}, bf16[136,256]{1,0:T(8,128)(2,1)S(1)}, u32[]{:S(2)}, u32[]{:S(2)}) collective-permute-start(bf16[136,256]{1,0:T(8,128)(2,1)S(1)} %shard_map.84.refs_0_), channel_id=1, source_target_pairs={{0,4},{4,0},{8,12},{12,8},{16,20},{20,16},{24,28},{28,24},{1,5},{5... | collective-permute-start | bytes 208904 | tf_op jit(solution)/shard_map/ppermute | solution.py:413
  41.7 4.6 %collective-permute-start.12 = (bf16[136,256]{1,0:T(8,128)(2,1)S(1)}, bf16[136,256]{1,0:T(8,128)(2,1)S(1)}, u32[]{:S(2)}, u32[]{:S(2)}) collective-permute-start(bf16[136,256]{1,0:T(8,128)(2,1)S(1)} %shard_map.84.refs_0_), channel_id=1, source_target_pairs={{0,8},{4,12},{8,0},{12,4},{16,24},{20,28},{24,16},{28,20},{1,9},{5... | collective-permute-start | bytes 208904 | tf_op jit(solution)/shard_map/ppermute | solution.py:413
  43.3 5.2 %collective-permute-start.13 = (bf16[136,256]{1,0:T(8,128)(2,1)S(1)}, bf16[136,256]{1,0:T(8,128)(2,1)S(1)}, u32[]{:S(2)}, u32[]{:S(2)}) collective-permute-start(bf16[136,256]{1,0:T(8,128)(2,1)S(1)} %shard_map.84.refs_0_), channel_id=1, source_target_pairs={{0,12},{4,8},{8,4},{12,0},{16,28},{20,24},{24,20},{28,16},{1,13},{... | collective-permute-start | bytes 208904 | tf_op jit(solution)/shard_map/ppermute | solution.py:413
  48.8 6.1 %collective-permute-start.14 = (bf16[144,256]{1,0:T(8,128)(2,1)S(1)}, bf16[144,256]{1,0:T(8,128)(2,1)S(1)}, u32[]{:S(2)}, u32[]{:S(2)}) collective-permute-start(bf16[144,256]{1,0:T(8,128)(2,1)S(1)} %get-tuple-element.42.mine), channel_id=1, source_target_pairs={{0,16},{4,20},{8,24},{12,28},{16,0},{20,4},{24,8},{28,12},{1,17},{... | collective-permute-start | bytes 221192 | tf_op jit(solution)/shard_map/ppermute | solution.py:419
